TPU v7x, 128 devices: a whole 4x4x4 slice. The times are simulated.
128 devices in a mesh: sp: 16 (over z, y), tp: 8 (over x, core).
Axes of the slice: x: 4, y: 4, z: 4, core: 2. Of those that a mesh axis runs over, the one named last changes fastest.
Arguments:
- stream: bfloat16 [6144, 2048], P(('sp', 'tp')), may hold values from -6 to 6
- query_nope: bfloat16 [6144, 16, 128], P('sp', 'tp'), may hold values from -6 to 6
- query_rope: bfloat16 [6144, 16, 64], P('sp', 'tp'), may hold values from -700 to 700
- latent: bfloat16 [6144, 512], P('sp'), may hold values from -6 to 6
- rope_key: bfloat16 [6144, 64], P('sp'), may hold values from -6 to 6
- latent_gain: float32 [512], replicated, may hold values from 0.1 to 1.9
- key_up: bfloat16 [512, 16, 128], P(None, 'tp'), may hold values from -0.375 to 0.375
- value_up: bfloat16 [512, 16, 128], P(None, 'tp'), may hold values from -2.6516504 to 2.6516504
- out_gain: float32 [2048], P('tp'), may hold values from 0.1 to 1.9
- out_weight: bfloat16 [2048, 2048], P('tp'), may hold values from -0.125 to 0.125
- norm_gain: float32 [2048], replicated, may hold values from 0.1 to 1.9
- ff_in: bfloat16 [2048, 8192], P('sp', 'tp'), may hold values from -0.125 to 0.125
- ff_out: bfloat16 [8192, 2048], P('tp', 'sp'), may hold values from -0.0625 to 0.0625
Outputs:
- layer_out: bfloat16 [6144, 2048], P(('sp', 'tp'))
All inputs are finite; a program needn't handle non-finite values.
Results may differ from a plain program's by a relative error of at most 0.018.
Values may be sent and summed in bfloat16 or wider, within the bound.
A program may use at most 128 MiB of HBM per device.

v0:
```python
import math

import jax
import jax.numpy as jnp
from jax import lax
from jax.sharding import PartitionSpec as P

HEADS = 16
NOPE = 128
ROPE = 64
LATENT = 512
VDIM = 128


EPS = 1e-06
THETA = 10000.0


def from_everyone(shard, axis):
    count = lax.axis_size(axis)
    return lax.all_to_all(
        jnp.broadcast_to(shard[None], (count, *shard.shape)), axis, 0, 0, tiled=True
    )


def over_copies(shard, axis):
    everything = from_everyone(shard, axis)
    return jnp.sum(everything, axis=0)


def cut_along(shard, dim, count):
    dims = shard.shape
    tiles = shard.reshape(*dims[:dim], count, dims[dim] // count, *dims[dim + 1 :])
    return jnp.moveaxis(tiles, dim, 0)


def sent_and_summed(shard, axis, dim):
    count = lax.axis_size(axis)
    tiles = lax.all_to_all(cut_along(shard, dim, count), axis, 0, 0, tiled=True)
    return jnp.sum(tiles.astype(jnp.float32), axis=0)


def joined_along(tiles, dim):
    tiles = jnp.moveaxis(tiles, 0, dim)
    dims = tiles.shape
    return tiles.reshape(*dims[:dim], dims[dim] * dims[dim + 1], *dims[dim + 2 :])


def collect(shard, axis, dim):
    tiles = from_everyone(shard, axis)
    return joined_along(tiles, dim)


def turn(values, positions):
    full_width = values.shape[-1]
    half_width = full_width // 2
    inverse = jnp.power(THETA, -jnp.arange(0, full_width, 2, dtype=jnp.float32) / full_width)
    angles = positions[:, None] * inverse[None, :]
    cosine = jnp.cos(angles)
    sine_part = jnp.sin(angles)
    if values.ndim == 3:
        cosine = cosine[:, None, :]
        sine_part = sine_part[:, None, :]
    vector = values.astype(jnp.float32)
    lower_half = vector[..., :half_width]
    upper_half = vector[..., half_width:]
    return jnp.concatenate(
        [
            lower_half * cosine - upper_half * sine_part,
            lower_half * sine_part + upper_half * cosine,
        ],
        axis=-1,
    )


def body(
    stream,
    query_nope,
    query_rope,
    latent,
    rope_key,
    latent_gain,
    key_up,
    value_up,
    out_gain,
    out_weight,
    norm_gain,
    ff_in,
    ff_out,
):
    local_rows = query_nope.shape[0]
    local_heads = query_nope.shape[1]
    row_start = lax.axis_index("sp") * local_rows
    positions = (row_start + jnp.arange(local_rows, dtype=jnp.int32)).astype(jnp.float32)
    lat_full = latent.astype(jnp.float32)
    normed = (
        lat_full
        * lax.rsqrt(jnp.mean(lat_full * lat_full, axis=-1, keepdims=True) + EPS)
        * latent_gain
    ).astype(jnp.bfloat16)
    keys_rot = turn(rope_key, positions).astype(jnp.bfloat16)
    query_rot = turn(query_rope, positions).astype(jnp.bfloat16)
    query_lat = jnp.einsum(
        "thn,lhn->thl", query_nope, key_up, preferred_element_type=jnp.float32
    ).astype(jnp.bfloat16)
    score_scale = 1.0 / math.sqrt(NOPE + ROPE)

    def fold_block(running, lat_block, rot_block):
        running_max, running_sum, accum = running
        scores = (
            jnp.einsum("thl,kl->thk", query_lat, lat_block, preferred_element_type=jnp.float32)
            + jnp.einsum("thr,kr->thk", query_rot, rot_block, preferred_element_type=jnp.float32)
        ) * score_scale
        new_max = jnp.maximum(running_max, jnp.max(scores, axis=-1))
        fading = jnp.exp(running_max - new_max)
        expo = jnp.exp(scores - new_max[..., None])
        running_sum = running_sum * fading + jnp.sum(expo, axis=-1)
        accum = accum * fading[..., None] + jnp.einsum(
            "thk,kl->thl", expo.astype(jnp.bfloat16), lat_block, preferred_element_type=jnp.float32
        )
        return (new_max, running_sum, accum)

    initial = (
        jnp.full((local_rows, local_heads), -1e30, jnp.float32),
        jnp.zeros((local_rows, local_heads), jnp.float32),
        jnp.zeros((local_rows, local_heads, LATENT), jnp.float32),
    )
    lat_piece = lax.all_gather(normed, "sp", axis=0, tiled=True)
    key_piece = lax.all_gather(keys_rot, "sp", axis=0, tiled=True)
    key_count = lat_piece.shape[0]
    key_block = math.gcd(key_count, 2048)
    lat_blocks = lat_piece.reshape(key_count // key_block, key_block, lat_piece.shape[1])
    key_blocks = key_piece.reshape(key_count // key_block, key_block, key_piece.shape[1])

    def advance(running, block_pair):
        return (fold_block(running, block_pair[0], block_pair[1]), None)

    result, _ = lax.scan(advance, initial, (lat_blocks, key_blocks))
    running_max, running_sum, accum = result
    out_lat = (accum / running_sum[..., None]).astype(jnp.bfloat16)
    head_out = jnp.einsum("thl,lhv->thv", out_lat, value_up, preferred_element_type=jnp.float32)
    square_sums = over_copies(jnp.sum(head_out * head_out, axis=(1, 2)), "tp")
    row_scale = lax.rsqrt(square_sums / (HEADS * VDIM) + EPS)
    gated = (head_out.reshape(local_rows, local_heads * VDIM) * out_gain).astype(jnp.bfloat16)
    row_share = local_rows // lax.axis_size("tp")
    projected = sent_and_summed(
        jnp.dot(gated, out_weight, preferred_element_type=jnp.float32).astype(jnp.bfloat16), "tp", 0
    )
    own_scale = lax.dynamic_slice_in_dim(row_scale, lax.axis_index("tp") * row_share, row_share, 0)
    mid_stream = stream.astype(jnp.float32) + own_scale[:, None] * projected
    ff_input = (
        mid_stream
        * lax.rsqrt(jnp.mean(mid_stream * mid_stream, axis=-1, keepdims=True) + EPS)
        * norm_gain
    ).astype(jnp.bfloat16)
    all_rows = collect(ff_input, "tp", 0)
    pre_act = jnp.dot(
        all_rows,
        lax.all_gather(ff_in, "sp", axis=0, tiled=True),
        preferred_element_type=jnp.float32,
    )
    activation = jnp.square(jax.nn.relu(pre_act)).astype(jnp.bfloat16)
    ff_whole = lax.all_gather(ff_out, "sp", axis=1, tiled=True)
    mixed = sent_and_summed(
        jnp.dot(activation, ff_whole, preferred_element_type=jnp.float32).astype(jnp.bfloat16),
        "tp",
        0,
    )
    return (mid_stream + mixed).astype(jnp.bfloat16)


def solution(mesh):
    placed = (
        P(("sp", "tp"), None),
        P("sp", "tp", None),
        P("sp", "tp", None),
        P("sp", None),
        P("sp", None),
        P(),
        P(None, "tp", None),
        P(None, "tp", None),
        P("tp"),
        P("tp", None),
        P(),
        P("sp", "tp"),
        P("tp", "sp"),
    )
    return jax.shard_map(
        body, mesh=mesh, in_specs=placed, out_specs=P(("sp", "tp"), None), check_vma=False
    )
```

profile of v0, /device:TPU:1, one launch (start us, length us, event | category | flops | bytes accessed | tf_op | source)
XLA Modules:
  0.0 230.9 jit_solution(9691018627300126583)
XLA Ops:
  12.3 26.1 %all_gather.13 = bf16[6144,64]{0,1:T(8,128)(2,1)S(1)} all-gather(bf16[384,64]{0,1:T(8,128)(2,1)S(1)} %pad_maximum_fusion.1), channel_id=1, replica_groups=mesh['sp'=16,'tp'=8] {'sp'}, dimensions={0}, use_global_device_ids=true | all-gather | bytes 835584 | tf_op jit(solution)/shard_map/all_gather | solution.py:129
  40.2 35.3 %all-gather.4.cloned.1.call-done = bf16[6144,512]{1,0:T(8,128)(2,1)} async-done(((bf16[384,512]{1,0:T(8,128)(2,1)}), bf16[6144,512]{1,0:T(8,128)(2,1)}) %all-gather.4.cloned.1.call-update) | async-done | bytes 6291472 | tf_op jit(solution)/shard_map/all_gather | solution.py:128
  75.5 50.5 %while.15 = (s32[]{:T(128)}, f32[384,2]{0,1:T(2,128)S(1)}, f32[384,2]{0,1:T(2,128)S(1)}, f32[384,2,512]{2,0,1:T(8,128)}, bf16[3,2048,512]{2,1,0:T(8,128)(2,1)}, ...) while((s32[]{:T(128)}, f32[384,2]{0,1:T(2,128)S(1)}, ...), condition=%wide.region_4.5_spmd.clone, body=%wide.region_1.4_spmd.clone.sunk | while | flops 3434745600 | bytes 65160332 | solution.py:138
  75.5 3.5 %fusion.56 = f32[2048,384,2]{1,0,2:T(8,128)S(1)} fusion(bf16[384,2,512]{2,0,1:T(8,128)(2,1)S(1)} %get-tuple-element.221, bf16[3,2048,512]{2,1,0:T(8,128)(2,1)} %get-tuple-element.220, s32[]{:T(128)} %get-tuple-element.206), kind=kOutput, calls=%fused_computation.9.clone.1 | convolution fusion | flops 1610612736 | bytes 9175552 | tf_op jit(solution)/shard_map/while/body/eval_jaxpr/thl,kl->thk/dot_general | solution.py:111
  78.9 3.7 %bitcast_reduce_fusion.2 = (f32[384,2]{0,1:T(2,128)S(1)}, f32[2048,384,2]{1,0,2:T(8,128)}) fusion(f32[2048,384,2]{1,0,2:T(8,128)S(1)} %fusion.56, bf16[384,2,64]{0,2,1:T(8,128)(2,1)S(1)} %get-tuple-element.223, bf16[3,2048,64]{1,2,0:T(8,128)(2,1)S(1)} %get-tuple-element.222, s32[]{:T(128)} %get-tuple-element.206), kind=kOutput, calls=%fused_computation.1.clone.1 | convolution fusion | flops 206044416 | bytes 12946436 | tf_op jit(solution)/shard_map/while/body/eval_jaxpr/thr,kr->thk/dot_general | solution.py:112
  82.6 3.8 %fusion.58 = f32[384,2]{0,1:T(2,128)S(1)} fusion(f32[2048,384,2]{1,0,2:T(8,128)} %get-tuple-element.193, f32[384,2]{0,1:T(2,128)S(1)} %fusion.57), kind=kLoop, calls=%fused_computation.5.clone.1 | loop fusion | flops 3144960 | bytes 6297600 | tf_op jit(solution)/shard_map/while/body/eval_jaxpr/reduce_sum | solution.py:117
  87.3 4.7 %fusion.60 = f32[384,2,512]{2,0,1:T(8,128)} fusion(f32[384,2,512]{2,0,1:T(8,128)} %get-tuple-element.209, bf16[3,2048,512]{2,1,0:T(8,128)(2,1)} %get-tuple-element.220, s32[]{:T(128)} %get-tuple-element.206, f32[2048,384,2]{1,0,2:T(8,128)S(1)} %copy-done.1, f32[384,2]{0,1:T(2,128)S(1)} %fusion.57, f32[384,2]{0,1:T(2,128)S(1)} %get-tuple-element.195, ...), kind=kOutput, calls=%fused_computation.14.clone.1 | convolution fusion | flops 1614938112 | bytes 11540993 | tf_op jit(solution)/shard_map/while/body/eval_jaxpr/thk,kl->thl/dot_general | solution.py:118
  92.0 3.5 %fusion.56 = f32[2048,384,2]{1,0,2:T(8,128)S(1)} fusion(bf16[384,2,512]{2,0,1:T(8,128)(2,1)S(1)} %get-tuple-element.221, bf16[3,2048,512]{2,1,0:T(8,128)(2,1)} %get-tuple-element.220, s32[]{:T(128)} %get-tuple-element.206), kind=kOutput, calls=%fused_computation.9.clone.1 | convolution fusion | flops 1610612736 | bytes 9175552 | tf_op jit(solution)/shard_map/while/body/eval_jaxpr/thl,kl->thk/dot_general | solution.py:111
  95.5 3.7 %bitcast_reduce_fusion.2 = (f32[384,2]{0,1:T(2,128)S(1)}, f32[2048,384,2]{1,0,2:T(8,128)}) fusion(f32[2048,384,2]{1,0,2:T(8,128)S(1)} %fusion.56, bf16[384,2,64]{0,2,1:T(8,128)(2,1)S(1)} %get-tuple-element.223, bf16[3,2048,64]{1,2,0:T(8,128)(2,1)S(1)} %get-tuple-element.222, s32[]{:T(128)} %get-tuple-element.206), kind=kOutput, calls=%fused_computation.1.clone.1 | convolution fusion | flops 206044416 | bytes 12946436 | tf_op jit(solution)/shard_map/while/body/eval_jaxpr/thr,kr->thk/dot_general | solution.py:112
  99.2 3.8 %fusion.58 = f32[384,2]{0,1:T(2,128)S(1)} fusion(f32[2048,384,2]{1,0,2:T(8,128)} %get-tuple-element.193, f32[384,2]{0,1:T(2,128)S(1)} %fusion.57), kind=kLoop, calls=%fused_computation.5.clone.1 | loop fusion | flops 3144960 | bytes 6297600 | tf_op jit(solution)/shard_map/while/body/eval_jaxpr/reduce_sum | solution.py:117
  103.8 5.1 %fusion.60 = f32[384,2,512]{2,0,1:T(8,128)} fusion(f32[384,2,512]{2,0,1:T(8,128)} %get-tuple-element.209, bf16[3,2048,512]{2,1,0:T(8,128)(2,1)} %get-tuple-element.220, s32[]{:T(128)} %get-tuple-element.206, f32[2048,384,2]{1,0,2:T(8,128)S(1)} %copy-done.1, f32[384,2]{0,1:T(2,128)S(1)} %fusion.57, f32[384,2]{0,1:T(2,128)S(1)} %get-tuple-element.195, ...), kind=kOutput, calls=%fused_computation.14.clone.1 | convolution fusion | flops 1614938112 | bytes 11540993 | tf_op jit(solution)/shard_map/while/body/eval_jaxpr/thk,kl->thl/dot_general | solution.py:118
  108.9 3.4 %fusion.56 = f32[2048,384,2]{1,0,2:T(8,128)S(1)} fusion(bf16[384,2,512]{2,0,1:T(8,128)(2,1)S(1)} %get-tuple-element.221, bf16[3,2048,512]{2,1,0:T(8,128)(2,1)} %get-tuple-element.220, s32[]{:T(128)} %get-tuple-element.206), kind=kOutput, calls=%fused_computation.9.clone.1 | convolution fusion | flops 1610612736 | bytes 9175552 | tf_op jit(solution)/shard_map/while/body/eval_jaxpr/thl,kl->thk/dot_general | solution.py:111
  112.3 3.7 %bitcast_reduce_fusion.2 = (f32[384,2]{0,1:T(2,128)S(1)}, f32[2048,384,2]{1,0,2:T(8,128)}) fusion(f32[2048,384,2]{1,0,2:T(8,128)S(1)} %fusion.56, bf16[384,2,64]{0,2,1:T(8,128)(2,1)S(1)} %get-tuple-element.223, bf16[3,2048,64]{1,2,0:T(8,128)(2,1)S(1)} %get-tuple-element.222, s32[]{:T(128)} %get-tuple-element.206), kind=kOutput, calls=%fused_computation.1.clone.1 | convolution fusion | flops 206044416 | bytes 12946436 | tf_op jit(solution)/shard_map/while/body/eval_jaxpr/thr,kr->thk/dot_general | solution.py:112
  116.0 3.9 %fusion.58 = f32[384,2]{0,1:T(2,128)S(1)} fusion(f32[2048,384,2]{1,0,2:T(8,128)} %get-tuple-element.193, f32[384,2]{0,1:T(2,128)S(1)} %fusion.57), kind=kLoop, calls=%fused_computation.5.clone.1 | loop fusion | flops 3144960 | bytes 6297600 | tf_op jit(solution)/shard_map/while/body/eval_jaxpr/reduce_sum | solution.py:117
  120.9 5.2 %fusion.60 = f32[384,2,512]{2,0,1:T(8,128)} fusion(f32[384,2,512]{2,0,1:T(8,128)} %get-tuple-element.209, bf16[3,2048,512]{2,1,0:T(8,128)(2,1)} %get-tuple-element.220, s32[]{:T(128)} %get-tuple-element.206, f32[2048,384,2]{1,0,2:T(8,128)S(1)} %copy-done.1, f32[384,2]{0,1:T(2,128)S(1)} %fusion.57, f32[384,2]{0,1:T(2,128)S(1)} %get-tuple-element.195, ...), kind=kOutput, calls=%fused_computation.14.clone.1 | convolution fusion | flops 1614938112 | bytes 11540993 | tf_op jit(solution)/shard_map/while/body/eval_jaxpr/thk,kl->thl/dot_general | solution.py:118
  128.5 5.1 %all-to-all-start = ((f32[8,1,384]{2,1,0:T(1,128)}), f32[8,1,384]{2,1,0:T(1,128)S(1)}, u32[]{:S(2)}, u32[]{:S(2)}) async-start(f32[8,1,384]{2,1,0:T(1,128)} %broadcast_in_dim.15), calls=%async_computation | async-start | bytes 24576 | tf_op jit(solution)/shard_map/all_to_all | solution.py:21
  135.6 2.8 %all-to-all-done = f32[8,1,384]{2,1,0:T(1,128)S(1)} async-done(((f32[8,1,384]{2,1,0:T(1,128)}), f32[8,1,384]{2,1,0:T(1,128)S(1)}, u32[]{:S(2)}, u32[]{:S(2)}) %all-to-all-start) | async-done | bytes 12320 | tf_op jit(solution)/shard_map/all_to_all | solution.py:21
  138.3 4.3 %all-to-all-start.1 = ((bf16[8,48,2048]{2,1,0:T(8,128)(2,1)}), bf16[8,48,2048]{2,1,0:T(8,128)(2,1)S(1)}, u32[]{:S(2)}, u32[]{:S(2)}) async-start(bf16[8,48,2048]{2,1,0:T(8,128)(2,1)} %bitcast.4), calls=%async_computation.1 | async-start | bytes 3145728 | tf_op jit(solution)/shard_map/all_to_all | solution.py:39
  142.8 20.5 %all-to-all-done.1 = bf16[8,48,2048]{2,1,0:T(8,128)(2,1)S(1)} async-done(((bf16[8,48,2048]{2,1,0:T(8,128)(2,1)}), bf16[8,48,2048]{2,1,0:T(8,128)(2,1)S(1)}, u32[]{:S(2)}, u32[]{:S(2)}) %all-to-all-start.1) | async-done | bytes 1572896 | tf_op jit(solution)/shard_map/all_to_all | solution.py:39
  165.2 4.4 %all-to-all-start.2 = ((bf16[8,48,2048]{2,1,0:T(8,128)(2,1)}), bf16[8,48,2048]{2,1,0:T(8,128)(2,1)S(1)}, u32[]{:S(2)}, u32[]{:S(2)}) async-start(bf16[8,48,2048]{2,1,0:T(8,128)(2,1)} %broadcast_in_dim.16), calls=%async_computation.2 | async-start | bytes 3145728 | tf_op jit(solution)/shard_map/all_to_all | solution.py:21
  169.7 16.7 %all-gather.8.cloned.1.call-done = bf16[1024,2048]{1,0:T(8,128)(2,1)} async-done(((bf16[1024,128]{1,0:T(8,128)(2,1)}), bf16[1024,2048]{1,0:T(8,128)(2,1)}) %all-gather.8.cloned.1.call-update) | async-done | bytes 4194320 | tf_op jit(solution)/shard_map/all_gather | solution.py:163
  186.4 3.9 %all-to-all-done.2 = bf16[8,48,2048]{2,1,0:T(8,128)(2,1)S(1)} async-done(((bf16[8,48,2048]{2,1,0:T(8,128)(2,1)}), bf16[8,48,2048]{2,1,0:T(8,128)(2,1)S(1)}, u32[]{:S(2)}, u32[]{:S(2)}) %all-to-all-start.2) | async-done | bytes 1572896 | tf_op jit(solution)/shard_map/all_to_all | solution.py:21
  190.3 8.0 %convolution_convert_fusion = bf16[384,2048]{1,0:T(8,128)(2,1)} fusion(bf16[1024,2048]{1,0:T(8,128)(2,1)} %all-gather.8.cloned.1.call-done, bf16[384,2048]{1,0:T(8,128)(2,1)S(1)} %bitcast.71, bf16[2048,1024]{1,0:T(8,128)(2,1)} %all-gather.6.cloned.1.call-done), kind=kOutput, calls=%fused_computation.27 | convolution fusion | flops 3223191552 | bytes 11534336 | tf_op jit(solution)/shard_map/dot_general | solution.py:165
  198.3 25.0 %all_to_all.21 = bf16[8,48,2048]{2,1,0:T(8,128)(2,1)S(1)} all-to-all(bf16[8,48,2048]{2,1,0:T(8,128)(2,1)} %bitcast.72), channel_id=1, replica_groups=mesh['sp'=16,'tp'=8] {'tp'}, dimensions={0} | all-to-all | bytes 3145728 | tf_op jit(solution)/shard_map/all_to_all | solution.py:39
  (71 shorter events, 17.5 us)
Async XLA Ops:
  6.5 127.3 %copy-start = (bf16[256,2048]{1,0:T(8,128)(2,1)S(1)}, bf16[256,2048]{1,0:T(8,128)(2,1)}, u32[]{:S(2)}) copy-start(bf16[256,2048]{1,0:T(8,128)(2,1)} %param.24) | copy-start | bytes 3145732
  6.5 4.8 %copy-start.6 = (bf16[384,64]{0,1:T(8,128)(2,1)S(1)}, bf16[384,64]{0,1:T(8,128)(2,1)}, u32[]{:S(2)}) copy-start(bf16[384,64]{0,1:T(8,128)(2,1)} %param.19) | copy-start | bytes 147460
  6.5 4.8 %copy-start.5 = (bf16[384,2,64]{0,2,1:T(8,128)(2,1)S(1)}, bf16[384,2,64]{0,2,1:T(8,128)(2,1)}, u32[]{:S(2)}) copy-start(bf16[384,2,64]{0,2,1:T(8,128)(2,1)} %param.17) | copy-start | bytes 294916
  6.5 68.9 %all-gather.4.cloned.1.call-start = ((), (), s32[]{:S(2)}) async-start(), calls=%async_computation.4 | async-start | bytes 6684672 | tf_op jit(solution)/shard_map/all_gather | solution.py:128
  9.7 28.8 %copy-start.3 = (bf16[512,2,128]{2,1,0:T(2,128)(2,1)S(1)}, bf16[512,2,128]{2,1,0:T(2,128)(2,1)}, u32[]{:S(2)}) copy-start(bf16[512,2,128]{2,1,0:T(2,128)(2,1)} %param.21) | copy-start | bytes 786436
  9.7 28.8 %copy-start.4 = (bf16[384,2,128]{2,1,0:T(2,128)(2,1)S(1)}, bf16[384,2,128]{2,1,0:T(2,128)(2,1)}, u32[]{:S(2)}) copy-start(bf16[384,2,128]{2,1,0:T(2,128)(2,1)} %param.16) | copy-start | bytes 589828
  9.7 160.0 %all-gather.6.cloned.1.call-start = ((), (), s32[]{:S(2)}) async-start(), calls=%async_computation.5 | async-start | bytes 4456448 | tf_op jit(solution)/shard_map/all_gather | solution.py:159
  10.5 175.9 %all-gather.8.cloned.1.call-start = ((), (), s32[]{:S(2)}) async-start(), calls=%async_computation.6 | async-start | bytes 4456448 | tf_op jit(solution)/shard_map/all_gather | solution.py:163
  75.5 50.6 %copy-start.9 = (bf16[512,2,128]{2,1,0:T(2,128)(2,1)S(1)}, bf16[512,2,128]{2,1,0:T(2,128)(2,1)}, u32[]{:S(2)}) copy-start(bf16[512,2,128]{2,1,0:T(2,128)(2,1)} %param.22) | copy-start | bytes 786436
  82.6 4.7 %copy-start.1 = (f32[2048,384,2]{1,0,2:T(8,128)S(1)}, f32[2048,384,2]{1,0,2:T(8,128)}, u32[]{:S(2)}) copy-start(f32[2048,384,2]{1,0,2:T(8,128)} %get-tuple-element.193) | copy-start | bytes 18874372 | tf_op jit(solution)/shard_map/while
  99.2 4.6 %copy-start.1 = (f32[2048,384,2]{1,0,2:T(8,128)S(1)}, f32[2048,384,2]{1,0,2:T(8,128)}, u32[]{:S(2)}) copy-start(f32[2048,384,2]{1,0,2:T(8,128)} %get-tuple-element.193) | copy-start | bytes 18874372 | tf_op jit(solution)/shard_map/while
  116.0 4.9 %copy-start.1 = (f32[2048,384,2]{1,0,2:T(8,128)S(1)}, f32[2048,384,2]{1,0,2:T(8,128)}, u32[]{:S(2)}) copy-start(f32[2048,384,2]{1,0,2:T(8,128)} %get-tuple-element.193) | copy-start | bytes 18874372 | tf_op jit(solution)/shard_map/while
  126.0 7.7 %copy-start.8 = (f32[256]{0:T(256)S(1)}, f32[256]{0:T(256)}, u32[]{:S(2)}) copy-start(f32[256]{0:T(256)} %param.23) | copy-start | bytes 3076
  128.5 9.8 %all-to-all-start = ((f32[8,1,384]{2,1,0:T(1,128)}), f32[8,1,384]{2,1,0:T(1,128)S(1)}, u32[]{:S(2)}, u32[]{:S(2)}) async-start(f32[8,1,384]{2,1,0:T(1,128)} %broadcast_in_dim.15), calls=%async_computation | async-start | bytes 24576 | tf_op jit(solution)/shard_map/all_to_all | solution.py:21
  138.3 25.2 %copy-start.2 = (bf16[48,2048]{1,0:T(8,128)(2,1)S(1)}, bf16[48,2048]{1,0:T(8,128)(2,1)}, u32[]{:S(2)}) copy-start(bf16[48,2048]{1,0:T(8,128)(2,1)} %param.15) | copy-start | bytes 589828
  138.3 25.4 %copy-start.7 = (f32[2048]{0:T(1024)S(1)}, f32[2048]{0:T(1024)}, u32[]{:S(2)}) copy-start(f32[2048]{0:T(1024)} %param.25) | copy-start | bytes 24580
  138.3 24.9 %all-to-all-start.1 = ((bf16[8,48,2048]{2,1,0:T(8,128)(2,1)}), bf16[8,48,2048]{2,1,0:T(8,128)(2,1)S(1)}, u32[]{:S(2)}, u32[]{:S(2)}) async-start(bf16[8,48,2048]{2,1,0:T(8,128)(2,1)} %bitcast.4), calls=%async_computation.1 | async-start | bytes 3145728 | tf_op jit(solution)/shard_map/all_to_all | solution.py:39
  165.2 25.1 %all-to-all-start.2 = ((bf16[8,48,2048]{2,1,0:T(8,128)(2,1)}), bf16[8,48,2048]{2,1,0:T(8,128)(2,1)S(1)}, u32[]{:S(2)}, u32[]{:S(2)}) async-start(bf16[8,48,2048]{2,1,0:T(8,128)(2,1)} %broadcast_in_dim.16), calls=%async_computation.2 | async-start | bytes 3145728 | tf_op jit(solution)/shard_map/all_to_all | solution.py:21
Sparse Core Ops, SparseCore 0:
  9.9 65.5 all-gather.3
  77.6 51.0 all-gather.5
  130.8 55.4 all-gather.7
where the time goes:
time: 232 us; the launch traced here: 231 us
  waiting for transfers between devices  80.6 us (35%)
  blocking collectives  51.1 us (22%)
  matrix products  48.4 us (21%)
  other arithmetic  18.5 us (8%)
  starting transfers between devices  14 us (6%)
  between operations  13.3 us (6%)
  local copies, waits for them, and re-layouts  5 us (2%)
    all_gather x1, waiting for transfers between devices, body(): lat_piece = lax.all_gather(normed, 'sp', axis=0, tiled=True)  35.3 us
    all_gather x1, blocking collectives, body(): key_piece = lax.all_gather(keys_rot, 'sp', axis=0, tiled=True)  26.1 us
    all_to_all x1, blocking collectives, sent_and_summed(): tiles = lax.all_to_all(cut_along(shard, dim, count), axis, 0, 0, tiled=True)  25 us
    all_to_all x1, waiting for transfers between devices, sent_and_summed(): tiles = lax.all_to_all(cut_along(shard, dim, count), axis, 0, 0, tiled=True)  20.5 us
    all_gather x1, waiting for transfers between devices, body(): ff_whole = lax.all_gather(ff_out, 'sp', axis=1, tiled=True)  16.7 us
    dot_general x3, matrix products, fold_block(): jnp.einsum('thk,kl->thl', expo.astype(jnp.bfloat16), lat_block, preferred...  15 us
    reduce_sum x3, other arithmetic, fold_block(): running_sum = running_sum * fading + jnp.sum(expo, axis=-1)  11.5 us
    dot_general x3, matrix products, fold_block(): jnp.einsum('thr,kr->thk', query_rot, rot_block, preferred_element_type=jn...  11.1 us
  transfers between devices with their start and end apart: 6, of which 5 were waited for; matrix products, arithmetic and copies ran while one was open for 25% of the time, Pallas kernels for 0%

commit v1 on v0

v1 whole, which is shorter than its diff:
```python
import math

import jax
import jax.numpy as jnp
import numpy as np
from jax import lax
from jax.experimental import pallas as pl
from jax.experimental.pallas import tpu as pltpu
from jax.sharding import PartitionSpec as P

MESH = pl.DeviceIdType.MESH
F32 = jnp.float32
BF16 = jnp.bfloat16

HEADS = 16
NOPE = 128
ROPE = 64
LATENT = 512
VDIM = 128
EPS = 1e-06
THETA = 10000.0

SIDE = 4
BLOCKS = SIDE * SIDE
ROWS = 384
OWN = 48
D = 2048
HID = 1024
PACK = 1152
PAIR = ROWS // 2
EXT = D + 128
UNIT = 4 * PAIR

YP, YM, ZP, ZM = (1, 0), (-1, 0), (0, 1), (0, -1)
LINKS = (YP, YM, ZP, ZM)


def wrap(v):
    return ((v[0] + 4) % 4, (v[1] + 4) % 4)


class Msg:
    def __init__(self, d, e, part, parent):
        self.d, self.e, self.part, self.parent = d, wrap(e), part, parent
        self.f = wrap((e[0] - d[0], e[1] - d[1]))
        self.level = 1 if parent is None else parent.level + 1
        self.kids = []
        self.id = None


def forwards(m):
    alongy = m.d[1] == 0
    first, cross = ("H0", (ZP, ZM)) if alongy else ("H1", (YP, YM))
    plus = m.d in (YP, ZP)
    out = []
    if m.part == "all":
        if plus:
            out.append((m.d, "a"))
        else:
            out += [(m.d, "H0b"), (m.d, "H1b")]
        out += [(c, first) for c in cross]
    elif m.level == 2 and m.part == "a":
        out += [(c, first + "a") for c in cross]
    elif m.level == 2 and m.part == first + "b":
        out += [(c, first + "b") for c in cross]
    elif m.level == 2 and m.part in ("H0", "H1"):
        out.append((m.d, m.part + ("a" if plus else "b")))
    elif m.level == 3 and m.parent.parent is not None and m.parent.level == 2 and m.parent.d != m.d:
        if m.part[2] == ("a" if plus else "b"):
            out.append((m.d, m.part))
    return out


def build_messages():
    todo = [Msg(d, (0, 0), "all", None) for d in LINKS]
    done = []
    while todo:
        m = todo.pop(0)
        m.id = len(done)
        done.append(m)
        m.kids = [Msg(d, m.f, part, m) for d, part in forwards(m)]
        todo += m.kids
    return done


MSGS = build_messages()
NMSG = len(MSGS)
LEVELS = [[m for m in MSGS if m.level == k] for k in (1, 2, 3, 4)]
ORDER = [(0, 0)]
_seen = {(0, 0): 4}
_quarters = {"all": "ABCD", "H0": "AB", "H1": "CD", "a": "BC", "H0b": "A", "H0a": "B", "H1a": "C", "H1b": "D"}
LAST = {}
for _m in MSGS:
    _seen[_m.f] = _seen.get(_m.f, 0) + len(_quarters[_m.part])
    if _seen[_m.f] == 4:
        ORDER.append(_m.f)
        LAST[_m.id] = _m.f
assert len(ORDER) == BLOCKS and all(v == 4 for v in _seen.values())
SLOT = {f: k for k, f in enumerate(ORDER)}


def parts_of(a, b, c, d):
    total = a + b + c + d
    return {
        "all": (0, total),
        "H0": (0, a + b),
        "H1": (a + b, c + d),
        "a": (a, b + c),
        "H0b": (0, a),
        "H0a": (a, b),
        "H1a": (a + b, c),
        "H1b": (a + b + c, d),
    }


LAT_PARTS = parts_of(16, 32, 16, 32)
IN_PARTS = parts_of(32, 32, 32, 32)
OUT_PARTS = parts_of(256, 256, 256, 256)


def rotary_tables():
    half = ROPE // 2
    inverse = np.power(THETA, -np.arange(0, ROPE, 2, dtype=np.float64) / ROPE)
    base = inverse[:, None] * np.arange(ROWS)[None, :]
    start = inverse[None, :] * (ROWS * np.arange(BLOCKS))[:, None]
    near = np.concatenate([np.cos(base), np.sin(base)], 0).astype(np.float32)
    far = np.concatenate([np.cos(start), np.sin(start)], 1).astype(np.float32)
    far = np.repeat(far[:, :, None], 128, axis=2)
    assert far.shape == (BLOCKS, 2 * half, 128)
    return near, far


def kernel(
    stream_in,
    qn,
    qr_t,
    latent,
    kr_t,
    lat_gain,
    key_up,
    value_up,
    out_gain,
    out_w_in,
    norm_gain,
    ff_in,
    ff_out,
    near,
    far_in,
    out,
    cat,
    w1,
    w2,
    qa,
    qb,
    sa,
    sb,
    pa,
    pb,
    acc,
    m_run,
    l_run,
    far,
    stream,
    out_w,
    proj,
    sib,
    xs,
    rx,
    fin,
    act,
    part,
    psib,
    pxs,
    prx,
    mid,
    fsum,
    loc_sem,
    ls,
    lr,
    s1,
    r1,
    s2,
    r2,
    ds,
    dr,
    ps,
    pr,
    fs,
    fr,
    gs,
    gr,
):
    sp = lax.axis_index("sp")
    tp = lax.axis_index("tp")
    z, y = sp // SIDE, sp % SIDE
    x, core = tp // 2, tp % 2
    other = 1 - core

    def at(f):
        return ((z + f[1]) % SIDE) * SIDE + (y + f[0]) % SIDE

    def torus(d):
        return (at(d), tp)

    sibling = (sp, x * 2 + other)

    def across(k):
        return (sp, ((x + k) % SIDE) * 2 + core)

    barrier = pltpu.get_barrier_semaphore()
    peers = [torus(d) for d in LINKS] + [sibling] + [across(k) for k in (1, 2, 3)]
    for peer in peers:
        pl.semaphore_signal(barrier, inc=1, device_id=peer, device_id_type=MESH)

    def local(src, dst, k):
        c = pltpu.make_async_copy(src, dst, loc_sem.at[k])
        c.start()
        return c

    far_copy = local(far_in.at[sp], far, 0)
    w1_copy = local(ff_in, w1.at[sp], 1)
    w2_copy = local(ff_out, w2.at[sp], 2)
    ow_copy = local(out_w_in, out_w, 3)
    st_copy = local(stream_in, stream, 4)

    def remote(src, dst, ssem, rsem, dev):
        return pltpu.make_async_remote_copy(
            src_ref=src, dst_ref=dst, send_sem=ssem, recv_sem=rsem, device_id=dev, device_id_type=MESH
        )

    def lat_view(f, part_name, whose):
        first, count = LAT_PARTS[part_name]
        start = SLOT[f] * PAIR + first + whose * (PAIR // 2)
        return cat.at[pl.ds(pl.multiple_of(start, 16), count), :]

    def lat_src(f, p):
        return lat_view(f, p, core)

    def in_view(f, p):
        first, count = IN_PARTS[p]
        return w1.at[at(f), pl.ds(first, count), :]

    def in_src(f, p):
        return ff_in if f == (0, 0) else in_view(f, p)

    def out_view(f, p):
        first, count = OUT_PARTS[p]
        return w2.at[at(f), pl.ds(first, count), :]

    def out_src(f, p):
        return ff_out if f == (0, 0) else out_view(f, p)

    gathers = {
        "L": (lat_src, lat_src, ls, lr),
        "W1": (in_src, in_view, s1, r1),
        "W2": (out_src, out_view, s2, r2),
    }

    def copy_of(g, m):
        src, view, ssem, rsem = gathers[g]
        if g == "L":
            first, count = LAT_PARTS[m.part]
            start = SLOT[m.f] * PAIR + first + core * (PAIR // 2)
            dst = cat.at[pl.ds(pl.multiple_of(start, 16), count), :]
        else:
            dst = view(m.e, m.part)
        return remote(src(m.e, m.part), dst, ssem.at[m.id], rsem.at[m.id], torus(m.d))

    def share(f):
        v = cat.at[pl.ds(pl.multiple_of(SLOT[f] * PAIR + core * (PAIR // 2), 32), PAIR // 2), :]
        return remote(v, v, ds.at[SLOT[f]], dr.at[SLOT[f]], sibling)

    def shared(f):
        v = cat.at[pl.ds(pl.multiple_of(SLOT[f] * PAIR + other * (PAIR // 2), 32), PAIR // 2), :]
        remote(v, v, ds.at[SLOT[f]], dr.at[SLOT[f]], sibling).wait_recv()

    def begin(g):
        for m in LEVELS[0]:
            copy_of(g, m).start()

    def receive(g, m):
        _, view, ssem, rsem = gathers[g]
        v = view(m.f, m.part)
        remote(v, v, ssem.at[m.id], rsem.at[m.id], torus(m.d)).wait_recv()
        for k in m.kids:
            copy_of(g, k).start()
        if g == "L" and m.id in LAST:
            share(LAST[m.id]).start()

    def level(g, k):
        for m in LEVELS[k - 1]:
            receive(g, m)

    lat = latent[...].astype(F32)
    normed = (
        lat * lax.rsqrt(jnp.mean(lat * lat, axis=-1, keepdims=True) + EPS) * lat_gain[...]
    ).astype(BF16)
    cat[0:PAIR, 0:LATENT] = normed[:PAIR]
    cat[0:PAIR, LATENT + 128 : PACK] = normed[PAIR:]
    far_copy.wait()
    half = ROPE // 2
    cos_n, sin_n = near[0:half, :], near[half:ROPE, :]
    cos_f = jnp.broadcast_to(far[0:half, 0:1], (half, ROWS))
    sin_f = jnp.broadcast_to(far[half:ROPE, 0:1], (half, ROWS))
    cosine = cos_n * cos_f - sin_n * sin_f
    sine = sin_n * cos_f + cos_n * sin_f

    def turned(v):
        low, high = v[:half].astype(F32), v[half:].astype(F32)
        a = low * cosine - high * sine
        b = low * sine + high * cosine
        return jnp.transpose(jnp.concatenate([a, b, a, b], axis=0))

    lane = lax.broadcasted_iota(jnp.int32, (ROWS, 128), 1)
    keys = turned(kr_t[...])
    cat[0:PAIR, LATENT : LATENT + 128] = jnp.where(
        lane[:PAIR] < ROPE, keys[:PAIR], keys[PAIR:]
    ).astype(BF16)

    pl.semaphore_wait(barrier, len(peers))
    begin("L")
    begin("W1")

    for h in range(2):
        rows = slice(h * ROWS, (h + 1) * ROWS)
        q_lat = lax.dot_general(
            qn[:, h * NOPE : (h + 1) * NOPE],
            key_up[:, h * NOPE : (h + 1) * NOPE],
            (((1,), (1,)), ((), ())),
            preferred_element_type=F32,
        ).astype(BF16)
        q_rot = turned(qr_t[h])
        qa[rows, 0:LATENT] = q_lat
        qa[rows, LATENT : LATENT + 128] = jnp.where(lane < ROPE, q_rot, 0.0).astype(BF16)
        qb[rows, 128 : LATENT + 128] = q_lat
        qb[rows, 0:128] = jnp.where(lane < ROPE, 0.0, q_rot).astype(BF16)

    acc[...] = jnp.zeros_like(acc)
    m_run[...] = jnp.full_like(m_run, -1e30)
    l_run[...] = jnp.zeros_like(l_run)
    factor = math.log2(math.e) / math.sqrt(NOPE + ROPE)

    def score(q, s, first):
        return lax.dot_general(
            q[...],
            cat[s * UNIT : (s + 1) * UNIT, first : first + LATENT + 128],
            (((1,), (1,)), ((), ())),
            preferred_element_type=F32,
        )

    def weigh(s_ref, p_ref, s, first):
        scores = s_ref[...]
        before = m_run[...]
        now = jnp.maximum(before, jnp.max(scores, axis=1, keepdims=True) * factor)
        fade = jnp.exp2(before - now)
        total = l_run[...] * fade
        for k in range(UNIT // 128):
            expo = jnp.exp2(scores[:, k * 128 : (k + 1) * 128] * factor - now)
            total = total + expo
            p_ref[:, k * 128 : (k + 1) * 128] = expo.astype(BF16)
        l_run[...] = total
        m_run[...] = now
        mixed = jnp.dot(
            p_ref[...],
            cat[s * UNIT : (s + 1) * UNIT, first : first + LATENT],
            preferred_element_type=F32,
        )
        for k in range(LATENT // 128):
            c = slice(k * 128, (k + 1) * 128)
            acc[:, c] = acc[:, c] * fade + mixed[:, c]

    def attend(s):
        sa[...] = score(qa, s, 0)
        sb[...] = score(qb, s, LATENT)
        weigh(sa, pa, s, 0)
        weigh(sb, pb, s, LATENT + 128)

    def need(first, last):
        for f in ORDER[first:last]:
            shared(f)

    level("L", 1)
    need(1, 4)
    attend(0)
    level("L", 2)
    level("W1", 1)
    need(4, 8)
    attend(1)
    level("L", 3)
    begin("W2")
    need(8, 12)
    attend(2)
    level("L", 4)
    level("W1", 2)
    need(12, 16)
    attend(3)
    level("W1", 3)

    out_lat = (acc[...] / jnp.sum(l_run[...], axis=1, keepdims=True)).astype(BF16)
    squares = jnp.zeros((ROWS, 1), F32)
    gated = []
    for h in range(2):
        c = slice(h * VDIM, (h + 1) * VDIM)
        head_out = jnp.dot(
            out_lat[h * ROWS : (h + 1) * ROWS], value_up[:, c], preferred_element_type=F32
        )
        squares = squares + jnp.sum(head_out * head_out, axis=1, keepdims=True)
        gated.append((head_out * out_gain[:, c]).astype(BF16))
    gated = jnp.concatenate(gated, axis=1)

    def two_terms(total, rows):
        high = total.astype(BF16).astype(F32)
        at_lane = lax.broadcasted_iota(jnp.int32, (rows, 128), 1)
        return jnp.where(at_lane == 0, high, jnp.where(at_lane == 1, total - high, 0.0)).astype(BF16)

    ow_copy.wait()
    tail = two_terms(squares, ROWS)
    for c in range(0, D, 512):
        piece = jnp.dot(gated, out_w[:, c : c + 512], preferred_element_type=F32).astype(BF16)
        proj[:, :, :, c : c + 512] = piece.reshape(SIDE, 2, OWN, 512)
    proj[:, :, :, D:EXT] = tail.reshape(SIDE, 2, OWN, 128)

    swap = remote(proj.at[:, other], sib, ps.at[0], pr.at[0], sibling)
    swap.start()
    swap.wait_recv()
    sends = [swap]

    def chip_sum(k):
        who = (x + k) % SIDE
        both = proj[who, core].astype(F32) + sib[who].astype(F32)
        total = jnp.sum(both[:, D:EXT], axis=1, keepdims=True)
        return both[:, :D], total

    for k in (1, 3, 2):
        body, total = chip_sum(k)
        xs[k - 1, :, 0:D] = body.astype(BF16)
        xs[k - 1, :, D:EXT] = two_terms(total, OWN)
        c = remote(xs.at[k - 1], rx.at[k - 1], ps.at[k], pr.at[k], across(k))
        c.start()
        sends.append(c)
    projected, total = chip_sum(0)
    level("W1", 4)
    level("W2", 1)
    for k in (1, 3, 2):
        remote(rx.at[k - 1], rx.at[k - 1], ps.at[k], pr.at[k], across(k)).wait_recv()
        projected = projected + rx[k - 1, :, 0:D].astype(F32)
        total = total + jnp.sum(rx[k - 1, :, D:EXT].astype(F32), axis=1, keepdims=True)
    row_scale = lax.rsqrt(total / (HEADS * VDIM) + EPS)
    st_copy.wait()
    middle = stream[...].astype(F32) + row_scale * projected
    mid[...] = middle
    ff_row = (
        middle
        * lax.rsqrt(jnp.mean(middle * middle, axis=-1, keepdims=True) + EPS)
        * norm_gain[...]
    ).astype(BF16)
    fin[tp] = ff_row

    def row_copy(k, to, src_tp):
        v = fin.at[src_tp]
        return remote(v, v, fs.at[k], fr.at[k], to)

    for k in (1, 3, 2):
        c = row_copy(k, across(k), tp)
        c.start()
        sends.append(c)
    c = row_copy(0, sibling, tp)
    c.start()
    sends.append(c)
    level("W2", 2)
    for k in (1, 3, 2):
        came = ((x + SIDE - k) % SIDE) * 2
        row_copy(k, across(k), came + core).wait_recv()
        c = row_copy(3 + k, sibling, came + core)
        c.start()
        sends.append(c)
    row_copy(0, sibling, x * 2 + other).wait_recv()
    for k in (1, 3, 2):
        came = ((x + SIDE - k) % SIDE) * 2
        row_copy(3 + k, sibling, came + other).wait_recv()

    w1_copy.wait()
    w2_copy.wait()
    rows = fin[...].reshape(ROWS, D)
    for c in range(0, HID, 256):
        pre = jnp.dot(
            rows, w1[:, :, c : c + 256].reshape(D, 256), preferred_element_type=F32
        )
        act[:, c : c + 256] = jnp.square(jnp.maximum(pre, 0.0)).astype(BF16)

    def swap_part(g):
        return remote(part.at[g, :, other], psib.at[g], gs.at[g, 0], gr.at[g, 0], sibling)

    def x_part(g, k):
        return remote(pxs.at[g, k - 1], prx.at[g, k - 1], gs.at[g, k], gr.at[g, k], across(k))

    def ff_group(g):
        for n, f in enumerate(ORDER[4 * g : 4 * g + 4]):
            piece = jnp.dot(act[...], w2[at(f)], preferred_element_type=F32).astype(BF16)
            part[g, :, :, :, n * 128 : (n + 1) * 128] = piece.reshape(SIDE, 2, OWN, 128)
        swap_part(g).start()

    def ff_chip(g):
        swap_part(g).wait_recv()
        for k in (1, 3, 2, 0):
            who = (x + k) % SIDE
            both = part[g, who, core].astype(F32) + psib[g, who].astype(F32)
            if k:
                pxs[g, k - 1] = both.astype(BF16)
                x_part(g, k).start()
            else:
                fsum[g] = both

    def ff_end(g):
        both = fsum[g]
        for k in (1, 3, 2):
            x_part(g, k).wait_recv()
            both = both + prx[g, k - 1].astype(F32)
        for n, f in enumerate(ORDER[4 * g : 4 * g + 4]):
            c = pl.ds(pl.multiple_of(at(f) * 128, 128), 128)
            out[:, c] = (mid[:, c] + both[:, n * 128 : (n + 1) * 128]).astype(BF16)

    ff_group(0)
    level("W2", 3)
    ff_group(1)
    ff_chip(0)
    level("W2", 4)
    ff_group(2)
    ff_chip(1)
    ff_group(3)
    ff_chip(2)
    ff_end(0)
    ff_chip(3)
    ff_end(1)
    ff_end(2)
    ff_end(3)

    for g in ("L", "W1", "W2"):
        for m in MSGS:
            copy_of(g, m).wait_send()
    for f in ORDER[1:]:
        share(f).wait_send()
    for c in sends:
        c.wait_send()
    for g in range(4):
        swap_part(g).wait_send()
        for k in (1, 2, 3):
            x_part(g, k).wait_send()


def body(
    stream,
    query_nope,
    query_rope,
    latent,
    rope_key,
    latent_gain,
    key_up,
    value_up,
    out_gain,
    out_weight,
    norm_gain,
    ff_in,
    ff_out,
):
    near, far = rotary_tables()
    vmem = pl.BlockSpec(memory_space=pltpu.VMEM)
    hbm = pl.BlockSpec(memory_space=pl.ANY)
    dma = pltpu.SemaphoreType.DMA
    return pl.pallas_call(
        kernel,
        out_shape=jax.ShapeDtypeStruct((OWN, D), BF16),
        in_specs=[hbm, vmem, vmem, vmem, vmem, vmem, vmem, vmem, vmem, hbm, vmem, hbm, hbm, vmem, hbm],
        out_specs=vmem,
        scratch_shapes=[
            pltpu.VMEM((BLOCKS * PAIR, PACK), BF16),
            pltpu.VMEM((BLOCKS, D // BLOCKS, HID), BF16),
            pltpu.VMEM((BLOCKS, HID, D // BLOCKS), BF16),
            pltpu.VMEM((2 * ROWS, LATENT + 128), BF16),
            pltpu.VMEM((2 * ROWS, LATENT + 128), BF16),
            pltpu.VMEM((2 * ROWS, UNIT), F32),
            pltpu.VMEM((2 * ROWS, UNIT), F32),
            pltpu.VMEM((2 * ROWS, UNIT), BF16),
            pltpu.VMEM((2 * ROWS, UNIT), BF16),
            pltpu.VMEM((2 * ROWS, LATENT), F32),
            pltpu.VMEM((2 * ROWS, 128), F32),
            pltpu.VMEM((2 * ROWS, 128), F32),
            pltpu.VMEM((ROPE, 128), F32),
            pltpu.VMEM((OWN, D), BF16),
            pltpu.VMEM((2 * VDIM, D), BF16),
            pltpu.VMEM((SIDE, 2, OWN, EXT), BF16),
            pltpu.VMEM((SIDE, OWN, EXT), BF16),
            pltpu.VMEM((SIDE - 1, OWN, EXT), BF16),
            pltpu.VMEM((SIDE - 1, OWN, EXT), BF16),
            pltpu.VMEM((2 * SIDE, OWN, D), BF16),
            pltpu.VMEM((ROWS, HID), BF16),
            pltpu.VMEM((4, SIDE, 2, OWN, 512), BF16),
            pltpu.VMEM((4, SIDE, OWN, 512), BF16),
            pltpu.VMEM((4, SIDE - 1, OWN, 512), BF16),
            pltpu.VMEM((4, SIDE - 1, OWN, 512), BF16),
            pltpu.VMEM((OWN, D), F32),
            pltpu.VMEM((4, OWN, 512), F32),
            dma((5,)),
            dma((NMSG,)),
            dma((NMSG,)),
            dma((NMSG,)),
            dma((NMSG,)),
            dma((NMSG,)),
            dma((NMSG,)),
            dma((BLOCKS,)),
            dma((BLOCKS,)),
            dma((4,)),
            dma((4,)),
            dma((7,)),
            dma((7,)),
            dma((4, 4)),
            dma((4, 4)),
        ],
        compiler_params=pltpu.CompilerParams(
            collective_id=0, has_side_effects=True, vmem_limit_bytes=60 * 1024 * 1024
        ),
    )(
        stream,
        query_nope.reshape(ROWS, 2 * NOPE),
        jnp.transpose(query_rope, (1, 2, 0)),
        latent,
        jnp.transpose(rope_key, (1, 0)),
        latent_gain.reshape(1, LATENT),
        key_up.reshape(LATENT, 2 * NOPE),
        value_up.reshape(LATENT, 2 * VDIM),
        out_gain.reshape(1, 2 * VDIM),
        out_weight,
        norm_gain.reshape(1, D),
        ff_in,
        ff_out,
        jnp.asarray(near),
        jnp.asarray(far),
    )


def solution(mesh):
    placed = (
        P(("sp", "tp"), None),
        P("sp", "tp", None),
        P("sp", "tp", None),
        P("sp", None),
        P("sp", None),
        P(),
        P(None, "tp", None),
        P(None, "tp", None),
        P("tp"),
        P("tp", None),
        P(),
        P("sp", "tp"),
        P("tp", "sp"),
    )
    return jax.shard_map(
        body, mesh=mesh, in_specs=placed, out_specs=P(("sp", "tp"), None), check_vma=False
    )
```

time: 232 us -> 106 us (0.46)
  Pallas kernels: 0 us -> 101 us
  waiting for transfers between devices: 80.6 us -> 0 us
  blocking collectives: 51.1 us -> 0 us
  matrix products: 48.4 us -> 0 us
  other arithmetic: 18.5 us -> 0 us
  starting transfers between devices: 14 us -> 0 us
  between operations: 13.3 us -> 0.01 us
    pallas_call x0 -> x1, Pallas kernels: none -> 101 us  [body(): pl.pallas_call(kernel, out_shape=jax.ShapeDtypeStruct((OWN, D), BF16), in...]
    all_gather x3 -> x0, waiting for transfers between devices: 52 us -> none  [the longest x1 35.3 us: body(): lat_piece = lax.all_gather(normed, 'sp', axis=0, tiled=True)]
    dot_general x13 -> x0, matrix products: 48.4 us -> none  [the longest x3 15 us: fold_block(): jnp.einsum('thk,kl->thl', expo.astype(jnp.bfloat16), lat_block, preferred...]
    all_to_all x3 -> x0, waiting for transfers between devices: 27.2 us -> none  [the longest x1 20.5 us: sent_and_summed(): tiles = lax.all_to_all(cut_along(shard, dim, count), axis, 0, 0, tiled=True)]
    all_gather x1 -> x0, blocking collectives: 26.1 us -> none  [body(): key_piece = lax.all_gather(keys_rot, 'sp', axis=0, tiled=True)]
    all_to_all x1 -> x0, blocking collectives: 25 us -> none  [sent_and_summed(): tiles = lax.all_to_all(cut_along(shard, dim, count), axis, 0, 0, tiled=True)]
    all_to_all x3 -> x0, starting transfers between devices: 13.9 us -> none  [the longest x2 9.59 us: from_everyone(): lax.all_to_all(jnp.broadcast_to(shard[None], (count, *shard.shape)), axis...]
    reduce_sum x8 -> x0, other arithmetic: 13.4 us -> none  [the longest x3 11.5 us: fold_block(): running_sum = running_sum * fading + jnp.sum(expo, axis=-1)]
  transfers between devices with their start and end apart: 6 -> 0, of which waited for: 5 -> 0; matrix products, arithmetic and copies ran while one was open for 25% -> 0% of each run, Pallas kernels for 0% -> 0%
where the time goes in v1:
time: 106 us
  Pallas kernels  101 us (95%)
  local copies, waits for them, and re-layouts  5.09 us (5%)
    pallas_call x1, Pallas kernels, body(): pl.pallas_call(kernel, out_shape=jax.ShapeDtypeStruct((OWN, D), BF16), in...  101 us
    unnamed x4, local copies, waits for them, and re-layouts  3.29 us

profile of v1, /device:TPU:1, one launch (start us, length us, event | category | flops | bytes accessed | tf_op | source)
XLA Modules:
  0.0 106.2 jit_solution(1669136249618095640)
XLA Ops:
  0.0 0.0 copy-start
  0.0 1.7 %copy.22 = bf16[48,8,2,128]{3,1,2,0:T(8,128)(2,1)} copy(bf16[48,8,2,128]{3,2,1,0:T(2,128)(2,1)} %bitcast.18) | data formatting | bytes 393216
  1.7 0.0 copy-done
  1.7 1.8 %copy_bitcast_fusion = (bf16[512,256]{1,0:T(8,128)(2,1)}, bf16[512,256]{1,0:T(8,128)(2,1)}) fusion(bf16[64,8,2,128]{3,2,1,0:T(2,128)(2,1)S(1)} %bitcast.16, bf16[64,8,2,128]{3,2,1,0:T(2,128)(2,1)} %bitcast.17), kind=kLoop, calls=%fused_computation | loop fusion | bytes 1048576 | tf_op jit(solution)/shard_map/reshape | solution.py:630
  3.5 101.1 %shard_map.145 = bf16[48,2048]{1,0:T(8,128)(2,1)} custom-call(bf16[48,2048]{1,0:T(8,128)(2,1)} %stream_in.1, bf16[384,256]{1,0:T(8,128)(2,1)} %bitcast.15, bf16[2,64,384]{2,1,0:T(8,128)(2,1)} %bitcast.19, bf16[384,512]{1,0:T(8,128)(2,1)} %latent.1, bf16[64,384]{1,0:T(8,128)(2,1)} %bitcast.20, f32[1,512]{1,0:T(1,128)} %bitcast.22, ...), custom_call_target="tpu_custom_call" | custom-call | tf_op jit(solution)/shard_map/pallas_call | solution.py:570
  104.6 1.6 %copy.24 = bf16[48,2048]{1,0:T(8,128)(2,1)} copy(bf16[48,2048]{1,0:T(8,128)(2,1)} %shard_map.145) | data formatting | bytes 393216
Async XLA Ops:
  0.0 1.7 %copy-start = (bf16[512,2,128]{2,1,0:T(2,128)(2,1)S(1)}, bf16[512,2,128]{2,1,0:T(2,128)(2,1)}, u32[]{:S(2)}) copy-start(bf16[512,2,128]{2,1,0:T(2,128)(2,1)} %param.22) | copy-start | bytes 786436

commit v2 on v1

--- a/solution.py
+++ b/solution.py
@@ -31,8 +31,8 @@
 EXT = D + 128
 UNIT = 4 * PAIR
 
-YP, YM, ZP, ZM = (1, 0), (-1, 0), (0, 1), (0, -1)
-LINKS = (YP, YM, ZP, ZM)
+UP, UM, VP, VM = (1, 0), (-1, 0), (0, 1), (0, -1)
+LINKS = (UP, UM, VP, VM)
 
 
 def wrap(v):
@@ -41,7 +41,7 @@
 
 class Msg:
     def __init__(self, d, e, part, parent):
-        self.d, self.e, self.part, self.parent = d, wrap(e), part, parent
+        self.d, self.e, self.part = d, wrap(e), part
         self.f = wrap((e[0] - d[0], e[1] - d[1]))
         self.level = 1 if parent is None else parent.level + 1
         self.kids = []
@@ -49,26 +49,14 @@
 
 
 def forwards(m):
-    alongy = m.d[1] == 0
-    first, cross = ("H0", (ZP, ZM)) if alongy else ("H1", (YP, YM))
-    plus = m.d in (YP, ZP)
-    out = []
-    if m.part == "all":
-        if plus:
-            out.append((m.d, "a"))
-        else:
-            out += [(m.d, "H0b"), (m.d, "H1b")]
-        out += [(c, first) for c in cross]
-    elif m.level == 2 and m.part == "a":
-        out += [(c, first + "a") for c in cross]
-    elif m.level == 2 and m.part == first + "b":
-        out += [(c, first + "b") for c in cross]
-    elif m.level == 2 and m.part in ("H0", "H1"):
-        out.append((m.d, m.part + ("a" if plus else "b")))
-    elif m.level == 3 and m.parent.parent is not None and m.parent.level == 2 and m.parent.d != m.d:
-        if m.part[2] == ("a" if plus else "b"):
-            out.append((m.d, m.part))
-    return out
+    plus = m.d in (UP, VP)
+    half = "a" if plus else "b"
+    if m.d[1] == 0:
+        across = [(VP, m.part), (VM, m.part)]
+        return ([(m.d, half)] if m.part == "all" else []) + across
+    if m.f[1] == 2 or m.part not in ("all", half):
+        return []
+    return [(m.d, half)]
 
 
 def build_messages():
@@ -87,35 +75,27 @@
 NMSG = len(MSGS)
 LEVELS = [[m for m in MSGS if m.level == k] for k in (1, 2, 3, 4)]
 ORDER = [(0, 0)]
-_seen = {(0, 0): 4}
-_quarters = {"all": "ABCD", "H0": "AB", "H1": "CD", "a": "BC", "H0b": "A", "H0a": "B", "H1a": "C", "H1b": "D"}
+_seen = {(0, 0): 2}
 LAST = {}
 for _m in MSGS:
-    _seen[_m.f] = _seen.get(_m.f, 0) + len(_quarters[_m.part])
-    if _seen[_m.f] == 4:
+    _seen[_m.f] = _seen.get(_m.f, 0) + (2 if _m.part == "all" else 1)
+    if _seen[_m.f] == 2:
         ORDER.append(_m.f)
         LAST[_m.id] = _m.f
-assert len(ORDER) == BLOCKS and all(v == 4 for v in _seen.values())
+assert len(ORDER) == BLOCKS and all(v == 2 for v in _seen.values())
 SLOT = {f: k for k, f in enumerate(ORDER)}
-
-
-def parts_of(a, b, c, d):
-    total = a + b + c + d
-    return {
-        "all": (0, total),
-        "H0": (0, a + b),
-        "H1": (a + b, c + d),
-        "a": (a, b + c),
-        "H0b": (0, a),
-        "H0a": (a, b),
-        "H1a": (a + b, c),
-        "H1b": (a + b + c, d),
-    }
-
-
-LAT_PARTS = parts_of(16, 32, 16, 32)
-IN_PARTS = parts_of(32, 32, 32, 32)
-OUT_PARTS = parts_of(256, 256, 256, 256)
+SLOTS_AT = [[SLOT[LAST[m.id]] for m in lev if m.id in LAST] for lev in LEVELS]
+COLUMNS = ORDER
+
+
+def parts_of(a, b):
+    return {"all": (0, a + b), "a": (0, a), "b": (a, b)}
+
+
+LAT_PARTS = parts_of(32, 32)
+IN_PARTS = parts_of(64, 64)
+OUT_PARTS = parts_of(512, 512)
+THIRD = 32
 
 
 def rotary_tables():
@@ -132,21 +112,28 @@
 
 def kernel(
     stream_in,
-    qn,
-    qr_t,
-    latent,
-    kr_t,
+    qn_in,
+    qr_in,
+    latent_in,
+    kr_in,
     lat_gain,
-    key_up,
-    value_up,
+    key_up_in,
+    value_up_in,
     out_gain,
     out_w_in,
     norm_gain,
     ff_in,
     ff_out,
-    near,
+    near_in,
     far_in,
     out,
+    qn,
+    qr_t,
+    latent,
+    kr_t,
+    key_up,
+    value_up,
+    near,
     cat,
     w1,
     w2,
@@ -174,6 +161,10 @@
     prx,
     mid,
     fsum,
+    wide,
+    wide2,
+    xls,
+    xlr,
     loc_sem,
     ls,
     lr,
@@ -196,11 +187,16 @@
     x, core = tp // 2, tp % 2
     other = 1 - core
 
+    odd = x % 2
+
+    def block_at(dy, dz):
+        return ((z + dz) % SIDE) * SIDE + (y + dy) % SIDE
+
     def at(f):
-        return ((z + f[1]) % SIDE) * SIDE + (y + f[0]) % SIDE
+        return block_at(f[0] * other + f[1] * core, f[0] * core + f[1] * other)
 
     def torus(d):
-        return (at(d), tp)
+        return (at(wrap(d)), tp)
 
     sibling = (sp, x * 2 + other)
 
@@ -217,7 +213,14 @@
         c.start()
         return c
 
-    far_copy = local(far_in.at[sp], far, 0)
+    early = [
+        local(latent_in, latent, 5),
+        local(far_in.at[sp], far, 0),
+        local(near_in, near, 6),
+        local(kr_in, kr_t, 7),
+    ]
+    early2 = [local(qn_in, qn, 8), local(key_up_in, key_up, 9), local(qr_in, qr_t, 10)]
+    vu_copy = local(value_up_in, value_up, 11)
     w1_copy = local(ff_in, w1.at[sp], 1)
     w2_copy = local(ff_out, w2.at[sp], 2)
     ow_copy = local(out_w_in, out_w, 3)
@@ -228,13 +231,12 @@
             src_ref=src, dst_ref=dst, send_sem=ssem, recv_sem=rsem, device_id=dev, device_id_type=MESH
         )
 
-    def lat_view(f, part_name, whose):
+    def lat_rows(slot, first, count):
+        return cat.at[pl.ds(pl.multiple_of(slot * PAIR + first, 32), count), :]
+
+    def lat_view(f, part_name):
         first, count = LAT_PARTS[part_name]
-        start = SLOT[f] * PAIR + first + whose * (PAIR // 2)
-        return cat.at[pl.ds(pl.multiple_of(start, 16), count), :]
-
-    def lat_src(f, p):
-        return lat_view(f, p, core)
+        return lat_rows(SLOT[f], core * (PAIR // 2) + odd * THIRD + first, count)
 
     def in_view(f, p):
         first, count = IN_PARTS[p]
@@ -251,28 +253,34 @@
         return ff_out if f == (0, 0) else out_view(f, p)
 
     gathers = {
-        "L": (lat_src, lat_src, ls, lr),
+        "L": (lat_view, lat_view, ls, lr),
         "W1": (in_src, in_view, s1, r1),
         "W2": (out_src, out_view, s2, r2),
     }
 
     def copy_of(g, m):
         src, view, ssem, rsem = gathers[g]
-        if g == "L":
-            first, count = LAT_PARTS[m.part]
-            start = SLOT[m.f] * PAIR + first + core * (PAIR // 2)
-            dst = cat.at[pl.ds(pl.multiple_of(start, 16), count), :]
-        else:
-            dst = view(m.e, m.part)
+        dst = view(m.f if g == "L" else m.e, m.part)
         return remote(src(m.e, m.part), dst, ssem.at[m.id], rsem.at[m.id], torus(m.d))
 
-    def share(f):
-        v = cat.at[pl.ds(pl.multiple_of(SLOT[f] * PAIR + core * (PAIR // 2), 32), PAIR // 2), :]
-        return remote(v, v, ds.at[SLOT[f]], dr.at[SLOT[f]], sibling)
-
-    def shared(f):
-        v = cat.at[pl.ds(pl.multiple_of(SLOT[f] * PAIR + other * (PAIR // 2), 32), PAIR // 2), :]
-        remote(v, v, ds.at[SLOT[f]], dr.at[SLOT[f]], sibling).wait_recv()
+    def along_x(slot):
+        v = lat_rows(slot, core * (PAIR // 2) + odd * 2 * THIRD, THIRD)
+        return remote(v, v, xls.at[slot], xlr.at[slot], across(1 if slot % 2 == 0 else 3))
+
+    def share(slot):
+        v = lat_rows(slot, core * (PAIR // 2), PAIR // 2)
+        return remote(v, v, ds.at[slot], dr.at[slot], sibling)
+
+    def pass_over(slots):
+        for slot in slots:
+            v = lat_rows(slot, core * (PAIR // 2) + (1 - odd) * 2 * THIRD, THIRD)
+            remote(v, v, xls.at[slot], xlr.at[slot], sibling).wait_recv()
+            share(slot).start()
+
+    def need(slots):
+        for slot in slots:
+            v = lat_rows(slot, other * (PAIR // 2), PAIR // 2)
+            remote(v, v, ds.at[slot], dr.at[slot], sibling).wait_recv()
 
     def begin(g):
         for m in LEVELS[0]:
@@ -285,19 +293,20 @@
         for k in m.kids:
             copy_of(g, k).start()
         if g == "L" and m.id in LAST:
-            share(LAST[m.id]).start()
+            along_x(SLOT[LAST[m.id]]).start()
 
     def level(g, k):
         for m in LEVELS[k - 1]:
             receive(g, m)
 
+    for c in early:
+        c.wait()
     lat = latent[...].astype(F32)
     normed = (
         lat * lax.rsqrt(jnp.mean(lat * lat, axis=-1, keepdims=True) + EPS) * lat_gain[...]
     ).astype(BF16)
     cat[0:PAIR, 0:LATENT] = normed[:PAIR]
     cat[0:PAIR, LATENT + 128 : PACK] = normed[PAIR:]
-    far_copy.wait()
     half = ROPE // 2
     cos_n, sin_n = near[0:half, :], near[half:ROPE, :]
     cos_f = jnp.broadcast_to(far[0:half, 0:1], (half, ROWS))
@@ -319,13 +328,16 @@
 
     pl.semaphore_wait(barrier, len(peers))
     begin("L")
-    begin("W1")
-
+
+    for c in early2:
+        c.wait()
+    wide[0 : 2 * ROWS, :] = qn[...].astype(F32)
+    wide2[...] = key_up[...].astype(F32)
     for h in range(2):
         rows = slice(h * ROWS, (h + 1) * ROWS)
         q_lat = lax.dot_general(
-            qn[:, h * NOPE : (h + 1) * NOPE],
-            key_up[:, h * NOPE : (h + 1) * NOPE],
+            wide[pl.ds(h, ROWS, stride=2), :].astype(BF16),
+            wide2[pl.ds(h, LATENT, stride=2), :].astype(BF16),
             (((1,), (1,)), ((), ())),
             preferred_element_type=F32,
         ).astype(BF16)
@@ -340,69 +352,74 @@
     l_run[...] = jnp.zeros_like(l_run)
     factor = math.log2(math.e) / math.sqrt(NOPE + ROPE)
 
-    def score(q, s, first):
+    def score(q, first_slot, slots, first):
         return lax.dot_general(
             q[...],
-            cat[s * UNIT : (s + 1) * UNIT, first : first + LATENT + 128],
+            cat[first_slot * PAIR : (first_slot + slots) * PAIR, first : first + LATENT + 128],
             (((1,), (1,)), ((), ())),
             preferred_element_type=F32,
         )
 
-    def weigh(s_ref, p_ref, s, first):
-        scores = s_ref[...]
+    def weigh(s_ref, p_ref, first_slot, slots, first):
+        keys_here = slots * PAIR
+        scores = s_ref[:, 0:keys_here]
         before = m_run[...]
         now = jnp.maximum(before, jnp.max(scores, axis=1, keepdims=True) * factor)
         fade = jnp.exp2(before - now)
         total = l_run[...] * fade
-        for k in range(UNIT // 128):
+        for k in range(keys_here // 128):
             expo = jnp.exp2(scores[:, k * 128 : (k + 1) * 128] * factor - now)
             total = total + expo
             p_ref[:, k * 128 : (k + 1) * 128] = expo.astype(BF16)
         l_run[...] = total
         m_run[...] = now
         mixed = jnp.dot(
-            p_ref[...],
-            cat[s * UNIT : (s + 1) * UNIT, first : first + LATENT],
+            p_ref[:, 0:keys_here],
+            cat[first_slot * PAIR : (first_slot + slots) * PAIR, first : first + LATENT],
             preferred_element_type=F32,
         )
         for k in range(LATENT // 128):
             c = slice(k * 128, (k + 1) * 128)
             acc[:, c] = acc[:, c] * fade + mixed[:, c]
 
-    def attend(s):
-        sa[...] = score(qa, s, 0)
-        sb[...] = score(qb, s, LATENT)
-        weigh(sa, pa, s, 0)
-        weigh(sb, pb, s, LATENT + 128)
-
-    def need(first, last):
-        for f in ORDER[first:last]:
-            shared(f)
+    def attend(first_slot, slots):
+        keys_here = slots * PAIR
+        sa[:, 0:keys_here] = score(qa, first_slot, slots, 0)
+        sb[:, 0:keys_here] = score(qb, first_slot, slots, LATENT)
+        weigh(sa, pa, first_slot, slots, 0)
+        weigh(sb, pb, first_slot, slots, LATENT + 128)
 
     level("L", 1)
-    need(1, 4)
-    attend(0)
     level("L", 2)
-    level("W1", 1)
-    need(4, 8)
-    attend(1)
+    begin("W1")
+    pass_over(SLOTS_AT[0])
+    need([1, 2, 3])
+    attend(0, 4)
+    pass_over(SLOTS_AT[1])
     level("L", 3)
     begin("W2")
-    need(8, 12)
-    attend(2)
+    need([4, 5, 6, 7])
+    attend(4, 4)
+    level("W1", 1)
     level("L", 4)
-    level("W1", 2)
-    need(12, 16)
-    attend(3)
-    level("W1", 3)
+    pass_over(SLOTS_AT[2])
+    need([8, 9, 10, 11])
+    attend(8, 4)
+    pass_over(SLOTS_AT[3])
+    need([12, 13, 14, 15])
+    attend(12, 4)
 
     out_lat = (acc[...] / jnp.sum(l_run[...], axis=1, keepdims=True)).astype(BF16)
+    vu_copy.wait()
+    wide2[...] = value_up[...].astype(F32)
     squares = jnp.zeros((ROWS, 1), F32)
     gated = []
     for h in range(2):
         c = slice(h * VDIM, (h + 1) * VDIM)
         head_out = jnp.dot(
-            out_lat[h * ROWS : (h + 1) * ROWS], value_up[:, c], preferred_element_type=F32
+            out_lat[h * ROWS : (h + 1) * ROWS],
+            wide2[pl.ds(h, LATENT, stride=2), :].astype(BF16),
+            preferred_element_type=F32,
         )
         squares = squares + jnp.sum(head_out * head_out, axis=1, keepdims=True)
         gated.append((head_out * out_gain[:, c]).astype(BF16))
@@ -439,7 +456,7 @@
         c.start()
         sends.append(c)
     projected, total = chip_sum(0)
-    level("W1", 4)
+    level("W1", 2)
     level("W2", 1)
     for k in (1, 3, 2):
         remote(rx.at[k - 1], rx.at[k - 1], ps.at[k], pr.at[k], across(k)).wait_recv()
@@ -468,6 +485,7 @@
     c.start()
     sends.append(c)
     level("W2", 2)
+    level("W1", 3)
     for k in (1, 3, 2):
         came = ((x + SIDE - k) % SIDE) * 2
         row_copy(k, across(k), came + core).wait_recv()
@@ -479,6 +497,8 @@
         came = ((x + SIDE - k) % SIDE) * 2
         row_copy(3 + k, sibling, came + other).wait_recv()
 
+    level("W2", 3)
+    level("W1", 4)
     w1_copy.wait()
     w2_copy.wait()
     rows = fin[...].reshape(ROWS, D)
@@ -495,8 +515,8 @@
         return remote(pxs.at[g, k - 1], prx.at[g, k - 1], gs.at[g, k], gr.at[g, k], across(k))
 
     def ff_group(g):
-        for n, f in enumerate(ORDER[4 * g : 4 * g + 4]):
-            piece = jnp.dot(act[...], w2[at(f)], preferred_element_type=F32).astype(BF16)
+        for n, f in enumerate(COLUMNS[4 * g : 4 * g + 4]):
+            piece = jnp.dot(act[...], w2[block_at(*f)], preferred_element_type=F32).astype(BF16)
             part[g, :, :, :, n * 128 : (n + 1) * 128] = piece.reshape(SIDE, 2, OWN, 128)
         swap_part(g).start()
 
@@ -516,12 +536,11 @@
         for k in (1, 3, 2):
             x_part(g, k).wait_recv()
             both = both + prx[g, k - 1].astype(F32)
-        for n, f in enumerate(ORDER[4 * g : 4 * g + 4]):
-            c = pl.ds(pl.multiple_of(at(f) * 128, 128), 128)
+        for n, f in enumerate(COLUMNS[4 * g : 4 * g + 4]):
+            c = pl.ds(pl.multiple_of(block_at(*f) * 128, 128), 128)
             out[:, c] = (mid[:, c] + both[:, n * 128 : (n + 1) * 128]).astype(BF16)
 
     ff_group(0)
-    level("W2", 3)
     ff_group(1)
     ff_chip(0)
     level("W2", 4)
@@ -538,8 +557,9 @@
     for g in ("L", "W1", "W2"):
         for m in MSGS:
             copy_of(g, m).wait_send()
-    for f in ORDER[1:]:
-        share(f).wait_send()
+    for slot in range(1, BLOCKS):
+        along_x(slot).wait_send()
+        share(slot).wait_send()
     for c in sends:
         c.wait_send()
     for g in range(4):
@@ -570,9 +590,16 @@
     return pl.pallas_call(
         kernel,
         out_shape=jax.ShapeDtypeStruct((OWN, D), BF16),
-        in_specs=[hbm, vmem, vmem, vmem, vmem, vmem, vmem, vmem, vmem, hbm, vmem, hbm, hbm, vmem, hbm],
+        in_specs=[hbm, hbm, hbm, hbm, hbm, vmem, hbm, hbm, vmem, hbm, vmem, hbm, hbm, hbm, hbm],
         out_specs=vmem,
         scratch_shapes=[
+            pltpu.VMEM((2 * ROWS, NOPE), BF16),
+            pltpu.VMEM((2, ROPE, ROWS), BF16),
+            pltpu.VMEM((ROWS, LATENT), BF16),
+            pltpu.VMEM((ROPE, ROWS), BF16),
+            pltpu.VMEM((2 * LATENT, NOPE), BF16),
+            pltpu.VMEM((2 * LATENT, VDIM), BF16),
+            pltpu.VMEM((ROPE, ROWS), F32),
             pltpu.VMEM((BLOCKS * PAIR, PACK), BF16),
             pltpu.VMEM((BLOCKS, D // BLOCKS, HID), BF16),
             pltpu.VMEM((BLOCKS, HID, D // BLOCKS), BF16),
@@ -600,7 +627,11 @@
             pltpu.VMEM((4, SIDE - 1, OWN, 512), BF16),
             pltpu.VMEM((OWN, D), F32),
             pltpu.VMEM((4, OWN, 512), F32),
-            dma((5,)),
+            pltpu.VMEM((2 * ROWS, NOPE), F32),
+            pltpu.VMEM((2 * LATENT, NOPE), F32),
+            dma((BLOCKS,)),
+            dma((BLOCKS,)),
+            dma((12,)),
             dma((NMSG,)),
             dma((NMSG,)),
             dma((NMSG,)),
@@ -621,13 +652,13 @@
         ),
     )(
         stream,
-        query_nope.reshape(ROWS, 2 * NOPE),
+        query_nope.reshape(2 * ROWS, NOPE),
         jnp.transpose(query_rope, (1, 2, 0)),
         latent,
         jnp.transpose(rope_key, (1, 0)),
         latent_gain.reshape(1, LATENT),
-        key_up.reshape(LATENT, 2 * NOPE),
-        value_up.reshape(LATENT, 2 * VDIM),
+        key_up.reshape(2 * LATENT, NOPE),
+        value_up.reshape(2 * LATENT, VDIM),
         out_gain.reshape(1, 2 * VDIM),
         out_weight,
         norm_gain.reshape(1, D),

time: 106 us -> 89.6 us (0.85)
  Pallas kernels: 101 us -> 87.8 us
  local copies, waits for them, and re-layouts: 5.09 us -> 1.62 us
    pallas_call x1, Pallas kernels: 101 us -> 87.8 us  [body(): pl.pallas_call(kernel, out_shape=jax.ShapeDtypeStruct((OWN, D), BF16), in...]
    reshape x1 -> x0, local copies, waits for them, and re-layouts: 1.8 us -> none  [body(): value_up.reshape(LATENT, 2 * VDIM)]
    unnamed x4 -> x1, local copies, waits for them, and re-layouts: 3.29 us -> 1.62 us
where the time goes in v2:
time: 89.6 us; the launch traced here: 89.4 us
  Pallas kernels  87.8 us (98%)
  local copies, waits for them, and re-layouts  1.62 us (2%)
    pallas_call x1, Pallas kernels, body(): pl.pallas_call(kernel, out_shape=jax.ShapeDtypeStruct((OWN, D), BF16), in...  87.8 us

profile of v2, /device:TPU:1, one launch (start us, length us, event | category | flops | bytes accessed | tf_op | source)
XLA Modules:
  0.0 89.4 jit_solution(15924070537256115192)
XLA Ops:
  0.0 87.8 %shard_map.145 = bf16[48,2048]{1,0:T(8,128)(2,1)} custom-call(bf16[48,2048]{1,0:T(8,128)(2,1)} %stream_in.1, bf16[768,128]{1,0:T(8,128)(2,1)} %bitcast.10, bf16[2,64,384]{2,1,0:T(8,128)(2,1)} %bitcast.11, bf16[384,512]{1,0:T(8,128)(2,1)} %latent_in.1, bf16[64,384]{1,0:T(8,128)(2,1)} %bitcast.12, f32[1,512]{1,0:T(1,128)} %bitcast.14, ...), custom_call_target="tpu_custom_call" | custom-call | tf_op jit(solution)/shard_map/pallas_call | solution.py:590
  87.8 1.6 %copy.17 = bf16[48,2048]{1,0:T(8,128)(2,1)} copy(bf16[48,2048]{1,0:T(8,128)(2,1)} %shard_map.145) | data formatting | bytes 393216

commit v3 on v2

v3 whole, which is shorter than its diff:
```python
import math

import jax
import jax.numpy as jnp
import numpy as np
from jax import lax
from jax.experimental import pallas as pl
from jax.experimental.pallas import tpu as pltpu
from jax.sharding import PartitionSpec as P

MESH = pl.DeviceIdType.MESH
F32 = jnp.float32
BF16 = jnp.bfloat16

HEADS = 16
NOPE = 128
ROPE = 64
LATENT = 512
VDIM = 128
EPS = 1e-06
THETA = 10000.0

SIDE = 4
BLOCKS = SIDE * SIDE
ROWS = 384
OWN = 48
D = 2048
HID = 1024
PACK = 1152
PAIR = ROWS // 2
EXT = D + 128
UNIT = 1024

UP, UM, VP, VM = (1, 0), (-1, 0), (0, 1), (0, -1)
LINKS = (UP, UM, VP, VM)


def wrap(v):
    return ((v[0] + 4) % 4, (v[1] + 4) % 4)


class Msg:
    def __init__(self, d, e, half, parent):
        self.d, self.e, self.half = d, wrap(e), half
        self.f = wrap((e[0] - d[0], e[1] - d[1]))
        self.level = 1 if parent is None else parent.level + 1
        self.kids = []
        self.id = None


def forwards(m):
    onward = m.d in ((UP, VP) if m.half == 0 else (UM, VM))
    if m.d[1] == 0:
        return ([m.d] if onward and m.f[0] != 2 else []) + [VP, VM]
    return [m.d] if onward and m.f[1] != 2 else []


def build_messages(half):
    todo = [Msg(d, (0, 0), half, None) for d in LINKS]
    done = []
    while todo:
        m = todo.pop(0)
        m.id = half * (BLOCKS - 1) + len(done)
        done.append(m)
        m.kids = [Msg(d, m.f, half, m) for d in forwards(m)]
        todo += m.kids
    return done


TREES = [build_messages(half) for half in (0, 1)]
assert all(sorted({m.f for m in t} | {(0, 0)}) == [(i, j) for i in range(4) for j in range(4)] for t in TREES)
NMSG = 2 * (BLOCKS - 1)
LEVELS = [[[m for m in t if m.level == k] for k in (1, 2, 3, 4)] for t in TREES]
ORDER = [(0, 0)] + [m.f for m in TREES[0]]
SLOT = {f: k for k, f in enumerate(ORDER)}

NEAR = 5
THIRD = PAIR // 6
DIRECT, OVER_X = {}, {}
SHARED = {k: 0 if k < 4 else 1 if k < 11 else 2 if k < 15 else 3 for k in range(1, 16)}
PASSED = {k: 0 if k < 11 else 1 if k < 15 else 2 for k in range(5, 16)}
_row = NEAR * PAIR
for _slots, _table, _rows in (
    (range(5, 11), DIRECT, 4 * THIRD),
    (range(11, 15), DIRECT, 4 * THIRD),
    (range(5, 11), OVER_X, 2 * THIRD),
    (range(15, 16), DIRECT, 4 * THIRD),
    (range(11, 15), OVER_X, 2 * THIRD),
    (range(15, 16), OVER_X, 2 * THIRD),
):
    for _slot in _slots:
        _table[_slot] = _row
        _row += _rows
assert _row == BLOCKS * PAIR

PARTS = ((0, 32), (32, 48))
EDGES = (0, 5, 11, 16)
GROUPS = len(EDGES) - 1


def rotary_tables():
    half = ROPE // 2
    inverse = np.power(THETA, -np.arange(0, ROPE, 2, dtype=np.float64) / ROPE)
    base = inverse[:, None] * np.arange(ROWS)[None, :]
    start = inverse[None, :] * (ROWS * np.arange(BLOCKS))[:, None]
    near = np.concatenate([np.cos(base), np.sin(base)], 0).astype(np.float32)
    far = np.concatenate([np.cos(start), np.sin(start)], 1).astype(np.float32)
    far = np.repeat(far[:, :, None], 128, axis=2)
    assert far.shape == (BLOCKS, 2 * half, 128)
    return near, far


def kernel(
    stream_in,
    qn_in,
    qr_in,
    latent_in,
    kr_in,
    lat_gain,
    key_up_in,
    value_up_in,
    out_gain,
    out_w_in,
    norm_gain,
    ff_in,
    ff_out,
    near_in,
    far_in,
    out,
    qn,
    qr_t,
    latent,
    kr_t,
    key_up,
    value_up,
    near,
    cat,
    w1,
    w2,
    qa,
    qb,
    sa,
    sb,
    pa,
    pb,
    acc,
    m_run,
    l_run,
    far,
    stream,
    out_w,
    proj,
    sib,
    xs,
    rx,
    fin,
    act,
    part,
    psib,
    pxs,
    prx,
    mid,
    fsum,
    sums,
    wide,
    wide2,
    er,
    xlr,
    xdr,
    loc_sem,
    ls,
    lr,
    s1,
    r1,
    s2,
    r2,
    dr,
    ps,
    pr,
    fr,
    gr,
):
    sp = lax.axis_index("sp")
    tp = lax.axis_index("tp")
    z, y = sp // SIDE, sp % SIDE
    x, core = tp // 2, tp % 2
    other = 1 - core


    def block_at(dy, dz):
        return ((z + dz) % SIDE) * SIDE + (y + dy) % SIDE

    def at(f):
        return block_at(f[0] * other + f[1] * core, f[0] * core + f[1] * other)

    def torus(d):
        return (at(wrap(d)), tp)

    sibling = (sp, x * 2 + other)

    def across(k):
        return (sp, ((x + k) % SIDE) * 2 + core)

    barrier = pltpu.get_barrier_semaphore()
    peers = [torus(d) for d in LINKS] + [sibling] + [across(k) for k in (1, 2, 3)]
    for peer in peers:
        pl.semaphore_signal(barrier, inc=1, device_id=peer, device_id_type=MESH)

    def local(src, dst, k):
        c = pltpu.make_async_copy(src, dst, loc_sem.at[k])
        c.start()
        return c

    early = [
        local(latent_in, latent, 5),
        local(far_in.at[sp], far, 0),
        local(near_in, near, 6),
        local(kr_in, kr_t, 7),
    ]
    early2 = [local(qn_in, qn, 8), local(key_up_in, key_up, 9), local(qr_in, qr_t, 10)]
    vu_copy = local(value_up_in, value_up, 11)
    w1_copy = local(ff_in, w1.at[sp], 1)
    w2_copy = local(ff_out, w2.at[sp], 2)
    ow_copy = local(out_w_in, out_w, 3)
    st_copy = local(stream_in, stream, 4)

    def remote(src, dst, ssem, rsem, dev):
        return pltpu.make_async_remote_copy(
            src_ref=src, dst_ref=dst, send_sem=ssem, recv_sem=rsem, device_id=dev, device_id_type=MESH
        )

    odd = x % 2

    def lat_rows(start, count):
        return cat.at[pl.ds(pl.multiple_of(start, 32), count), :]

    def lat_view(f, half):
        slot = SLOT[f]
        if slot < NEAR:
            return lat_rows(slot * PAIR + core * 3 * THIRD + (odd + half) * THIRD, THIRD)
        return lat_rows(DIRECT[slot] + core * 2 * THIRD + half * THIRD, THIRD)

    def rest_view(f):
        return lat_rows(SLOT[f] * PAIR + core * 3 * THIRD + (1 - odd) * 2 * THIRD, THIRD)

    def rest_copy(n):
        m = LEVELS[0][0][n]
        return remote(rest_view(m.e), rest_view(m.f), ls.at[0], er.at[0], torus(m.d))

    def in_view(f, half):
        return w1.at[at(f), pl.ds(half * 64, 64), :]

    def in_src(f, half):
        return ff_in.at[pl.ds(half * 64, 64), :] if f == (0, 0) else in_view(f, half)

    def out_view(f, half):
        return w2.at[at(f), pl.ds(half * 512, 512), :]

    def out_src(f, half):
        return ff_out.at[pl.ds(half * 512, 512), :] if f == (0, 0) else out_view(f, half)

    gathers = {
        "L": (lat_view, lat_view, ls, lr),
        "W1": (in_src, in_view, s1, r1),
        "W2": (out_src, out_view, s2, r2),
    }

    def copy_of(g, m):
        src, view, ssem, rsem = gathers[g]
        dst = view(m.f if g == "L" else m.e, m.half)
        k = m.id if g == "L" else m.half * 4 + m.level - 1
        return remote(src(m.e, m.half), dst, ssem.at[0], rsem.at[k], torus(m.d))

    def direct_rows(slot, who):
        if slot < NEAR:
            return lat_rows(slot * PAIR + who * 3 * THIRD, 3 * THIRD)
        return lat_rows(DIRECT[slot] + who * 2 * THIRD, 2 * THIRD)

    def x_rows(slot, who):
        return lat_rows(OVER_X[slot] + who * THIRD, THIRD)

    def share(slot):
        v = direct_rows(slot, core)
        return remote(v, v, ls.at[0], dr.at[SHARED[slot]], sibling)

    def share_x(slot):
        v = x_rows(slot, core)
        return remote(v, v, ls.at[0], xdr.at[PASSED[slot]], sibling)

    def along_x(slot):
        src = lat_rows(DIRECT[slot] + core * 2 * THIRD + odd * THIRD, THIRD)
        to = across(1 if slot % 2 == 0 else 3)
        return remote(src, x_rows(slot, core), ls.at[0], xlr.at[PASSED[slot]], to)

    def await_rows(count, sem):
        v = cat.at[pl.ds(0, count), :]
        remote(v, v, ls.at[0], sem, sibling).wait_recv()

    def pass_over(group):
        slots = [k for k in PASSED if PASSED[k] == group]
        await_rows(THIRD * len(slots), xlr.at[group])
        for slot in slots:
            share_x(slot).start()

    def need(direct, over):
        for group in direct:
            await_rows(
                sum((3 if k < NEAR else 2) * THIRD for k in SHARED if SHARED[k] == group), dr.at[group]
            )
        for group in over:
            await_rows(sum(THIRD for k in PASSED if PASSED[k] == group), xdr.at[group])

    def rest():
        await_rows(len(LINKS) * THIRD, er.at[0])
        for m in LEVELS[0][0]:
            share(SLOT[m.f]).start()

    def begin(g, half):
        for m in LEVELS[half][0]:
            copy_of(g, m).start()

    landed = {}

    def level(g, half, k):
        src, view, ssem, rsem = gathers[g]
        here = LEVELS[half][k - 1]
        if g != "L":
            whole = w1 if g == "W1" else w2
            tall = whole.shape[1] // 2
            if len(here) % 2:
                v = whole.at[0, pl.ds(0, tall), :]
            else:
                v = whole.at[pl.ds(0, len(here) // 2)]
            remote(v, v, ssem.at[0], rsem.at[half * 4 + k - 1], sibling).wait_recv()
        for m in here:
            if g == "L":
                v = view(m.f, half)
                remote(v, v, ssem.at[0], rsem.at[m.id], sibling).wait_recv()
            for kid in m.kids:
                copy_of(g, kid).start()
            if g == "L":
                landed[m.f] = landed.get(m.f, 0) + 1
                if landed[m.f] == 2 and k > 1:
                    along_x(SLOT[m.f]).start()
                    share(SLOT[m.f]).start()

    for c in early:
        c.wait()
    lat = latent[...].astype(F32)
    normed = (
        lat * lax.rsqrt(jnp.mean(lat * lat, axis=-1, keepdims=True) + EPS) * lat_gain[...]
    ).astype(BF16)
    cat[0:PAIR, 0:LATENT] = normed[:PAIR]
    cat[0:PAIR, LATENT + 128 : PACK] = normed[PAIR:]
    half = ROPE // 2
    cos_n, sin_n = near[0:half, :], near[half:ROPE, :]
    cos_f = jnp.broadcast_to(far[0:half, 0:1], (half, ROWS))
    sin_f = jnp.broadcast_to(far[half:ROPE, 0:1], (half, ROWS))
    cosine = cos_n * cos_f - sin_n * sin_f
    sine = sin_n * cos_f + cos_n * sin_f

    def turned(v):
        low, high = v[:half].astype(F32), v[half:].astype(F32)
        a = low * cosine - high * sine
        b = low * sine + high * cosine
        return jnp.transpose(jnp.concatenate([a, b, a, b], axis=0))

    lane = lax.broadcasted_iota(jnp.int32, (ROWS, 128), 1)
    keys = turned(kr_t[...])
    cat[0:PAIR, LATENT : LATENT + 128] = jnp.where(
        lane[:PAIR] < ROPE, keys[:PAIR], keys[PAIR:]
    ).astype(BF16)

    pl.semaphore_wait(barrier, len(peers))
    begin("L", 0)
    begin("L", 1)
    for n in range(len(LINKS)):
        rest_copy(n).start()

    for c in early2:
        c.wait()
    wide[0 : 2 * ROWS, :] = qn[...].astype(F32)
    wide2[...] = key_up[...].astype(F32)
    for h in range(2):
        rows = slice(h * ROWS, (h + 1) * ROWS)
        q_lat = lax.dot_general(
            wide[pl.ds(h, ROWS, stride=2), :].astype(BF16),
            wide2[pl.ds(h, LATENT, stride=2), :].astype(BF16),
            (((1,), (1,)), ((), ())),
            preferred_element_type=F32,
        ).astype(BF16)
        q_rot = turned(qr_t[h])
        qa[rows, 0:LATENT] = q_lat
        qa[rows, LATENT : LATENT + 128] = jnp.where(lane < ROPE, q_rot, 0.0).astype(BF16)
        qb[rows, 128 : LATENT + 128] = q_lat
        qb[rows, 0:128] = jnp.where(lane < ROPE, 0.0, q_rot).astype(BF16)

    acc[...] = jnp.zeros_like(acc)
    m_run[...] = jnp.full_like(m_run, -1e30)
    l_run[...] = jnp.zeros_like(l_run)
    factor = math.log2(math.e) / math.sqrt(NOPE + ROPE)

    def score(q, row, count, first):
        return lax.dot_general(
            q[...],
            cat[row : row + count, first : first + LATENT + 128],
            (((1,), (1,)), ((), ())),
            preferred_element_type=F32,
        )

    def weigh(s_ref, p_ref, row, count, first):
        scores = s_ref[:, 0:count]
        before = m_run[...]
        now = jnp.maximum(before, jnp.max(scores, axis=1, keepdims=True) * factor)
        fade = jnp.exp2(before - now)
        total = l_run[...] * fade
        for k in range(count // 128):
            expo = jnp.exp2(scores[:, k * 128 : (k + 1) * 128] * factor - now)
            total = total + expo
            p_ref[:, k * 128 : (k + 1) * 128] = expo.astype(BF16)
        l_run[...] = total
        m_run[...] = now
        mixed = jnp.dot(
            p_ref[:, 0:count],
            cat[row : row + count, first : first + LATENT],
            preferred_element_type=F32,
        )
        for k in range(LATENT // 128):
            c = slice(k * 128, (k + 1) * 128)
            acc[:, c] = acc[:, c] * fade + mixed[:, c]

    def attend(row, count, between=()):
        sa[:, 0:count] = score(qa, row, count, 0)
        sb[:, 0:count] = score(qb, row, count, LATENT)
        weigh(sa, pa, row, count, 0)
        for g, half, k in between:
            level(g, half, k)
        weigh(sb, pb, row, count, LATENT + 128)

    level("L", 0, 1)
    level("L", 1, 1)
    begin("W1", 0)
    rest()
    need([0], [])
    attend(0, 768)
    level("L", 0, 2)
    level("L", 1, 2)
    begin("W1", 1)
    need([1], [])
    attend(768, 768)
    level("L", 0, 3)
    level("L", 1, 3)
    level("W1", 0, 1)
    begin("W2", 0)
    pass_over(0)
    need([2], [0])
    attend(1536, 1024, [("L", 0, 4), ("L", 1, 4), ("W1", 1, 1)])
    begin("W2", 1)
    pass_over(1)
    pass_over(2)
    need([3], [1, 2])
    attend(2560, 512, [("W1", 0, 2)])

    out_lat = (acc[...] / jnp.sum(l_run[...], axis=1, keepdims=True)).astype(BF16)
    vu_copy.wait()
    wide2[...] = value_up[...].astype(F32)
    squares = jnp.zeros((ROWS, 1), F32)
    gated = []
    for h in range(2):
        c = slice(h * VDIM, (h + 1) * VDIM)
        head_out = jnp.dot(
            out_lat[h * ROWS : (h + 1) * ROWS],
            wide2[pl.ds(h, LATENT, stride=2), :].astype(BF16),
            preferred_element_type=F32,
        )
        squares = squares + jnp.sum(head_out * head_out, axis=1, keepdims=True)
        gated.append((head_out * out_gain[:, c]).astype(BF16))
    gated = jnp.concatenate(gated, axis=1)

    def two_terms(total, rows):
        high = total.astype(BF16).astype(F32)
        at_lane = lax.broadcasted_iota(jnp.int32, (rows, 128), 1)
        return jnp.where(at_lane == 0, high, jnp.where(at_lane == 1, total - high, 0.0)).astype(BF16)

    ow_copy.wait()
    tail = two_terms(squares, ROWS)
    for c in range(0, D, 512):
        piece = jnp.dot(gated, out_w[:, c : c + 512], preferred_element_type=F32).astype(BF16)
        proj[:, :, :, c : c + 512] = piece.reshape(SIDE, 2, OWN, 512)
    proj[:, :, :, D:EXT] = tail.reshape(SIDE, 2, OWN, 128)

    def rows_of(p):
        return pl.ds(PARTS[p][0], PARTS[p][1] - PARTS[p][0])

    def swap(p):
        r = rows_of(p)
        return remote(proj.at[:, other, r, :], sib.at[:, r, :], ps.at[0], pr.at[p, 0], sibling)

    def x_copy(p, k):
        r = rows_of(p)
        return remote(xs.at[k - 1, r, :], rx.at[k - 1, r, :], ps.at[1], pr.at[p, 1], across(k))

    def chip_send(p):
        first, last = PARTS[p]
        r = slice(first, last)
        swap(p).wait_recv()
        for k in (2, 1, 3, 0):
            who = (x + k) % SIDE
            both = proj[who, core, r, :].astype(F32) + sib[who, r, :].astype(F32)
            total = jnp.sum(both[:, D:EXT], axis=1, keepdims=True)
            if k:
                xs[k - 1, r, 0:D] = both[:, :D].astype(BF16)
                xs[k - 1, r, D:EXT] = two_terms(total, last - first)
                x_copy(p, k).start()
            else:
                mid[r, :] = both[:, :D]
                sums[r, :] = jnp.broadcast_to(total, (last - first, 128))

    def row_copy(p, k, to, src_tp):
        v = fin.at[src_tp, rows_of(p), :]
        return remote(v, v, ps.at[2], fr.at[p, k if 1 <= k <= 3 else 0], to)

    def came_from(k):
        return ((x + SIDE - k) % SIDE) * 2

    def mid_rows(p):
        r = slice(*PARTS[p])
        projected = mid[r, :]
        total = sums[r, 0:1]
        came = rx.at[:, rows_of(p), :]
        remote(came, came, ps.at[1], pr.at[p, 1], sibling).wait_recv()
        for k in (1, 3, 2):
            projected = projected + rx[k - 1, r, 0:D].astype(F32)
            total = total + jnp.sum(rx[k - 1, r, D:EXT].astype(F32), axis=1, keepdims=True)
        row_scale = lax.rsqrt(total / (HEADS * VDIM) + EPS)
        middle = stream[r, :].astype(F32) + row_scale * projected
        mid[r, :] = middle
        fin[tp, r, :] = (
            middle
            * lax.rsqrt(jnp.mean(middle * middle, axis=-1, keepdims=True) + EPS)
            * norm_gain[...]
        ).astype(BF16)
        for k in (2, 1, 3):
            row_copy(p, k, across(k), tp).start()
        row_copy(p, 0, sibling, tp).start()

    def spread(p):
        for k in (1, 3, 2):
            row_copy(p, k, across(k), came_from(k) + core).wait_recv()
            row_copy(p, 3 + k, sibling, came_from(k) + core).start()

    def spread_end(p):
        v = fin.at[pl.ds(0, SIDE), rows_of(p), :]
        remote(v, v, ps.at[2], fr.at[p, 0], sibling).wait_recv()

    def ff_in_half(p):
        first, last = PARTS[p]
        rows = fin[:, first:last, :].reshape(8 * (last - first), D)
        for c in range(0, HID, 256):
            pre = jnp.dot(
                rows, w1[:, :, c : c + 256].reshape(D, 256), preferred_element_type=F32
            )
            act[8 * first : 8 * last, c : c + 256] = jnp.square(jnp.maximum(pre, 0.0)).astype(BF16)

    def columns_of(g):
        return pl.ds(EDGES[g] * 128, (EDGES[g + 1] - EDGES[g]) * 128)

    def swap_part(g, p):
        r, c = rows_of(p), columns_of(g)
        return remote(
            part.at[:, other, r, c], psib.at[:, r, c], ps.at[3], gr.at[g, p, 0], sibling
        )

    def x_part(g, p, k):
        r, c = rows_of(p), columns_of(g)
        return remote(
            pxs.at[k - 1, r, c], prx.at[k - 1, r, c], ps.at[4], gr.at[g, p, 1], across(k)
        )

    def ff_group(g, p):
        first, last = PARTS[p]
        for n in range(EDGES[g], EDGES[g + 1]):
            f = ORDER[n]
            piece = jnp.dot(
                act[8 * first : 8 * last, :], w2[block_at(*f)], preferred_element_type=F32
            ).astype(BF16)
            part[:, :, first:last, n * 128 : (n + 1) * 128] = piece.reshape(
                SIDE, 2, last - first, 128
            )
        swap_part(g, p).start()

    def ff_chip(g, p):
        r, c = slice(*PARTS[p]), slice(EDGES[g] * 128, EDGES[g + 1] * 128)
        swap_part(g, p).wait_recv()
        for k in (2, 1, 3, 0):
            who = (x + k) % SIDE
            both = part[who, core, r, c].astype(F32) + psib[who, r, c].astype(F32)
            if k:
                pxs[k - 1, r, c] = both.astype(BF16)
                x_part(g, p, k).start()
            else:
                fsum[r, c] = both

    def ff_end(g, p):
        r = slice(*PARTS[p])
        came = prx.at[:, rows_of(p), columns_of(g)]
        remote(came, came, ps.at[4], gr.at[g, p, 1], sibling).wait_recv()
        for n in range(EDGES[g], EDGES[g + 1]):
            here = slice(n * 128, (n + 1) * 128)
            both = fsum[r, here]
            for k in (1, 3, 2):
                both = both + prx[k - 1, r, here].astype(F32)
            c = pl.ds(pl.multiple_of(block_at(*ORDER[n]) * 128, 128), 128)
            out[r, c] = (mid[r, c] + both).astype(BF16)

    def sent(v, sem):
        remote(v, v, sem, sem, sibling).wait_send()

    swap(0).start()
    swap(1).start()
    level("W1", 1, 2)
    level("W2", 0, 1)
    chip_send(0)
    chip_send(1)
    level("W2", 1, 1)
    st_copy.wait()
    w1_copy.wait()
    w2_copy.wait()
    level("W1", 0, 3)
    level("W1", 1, 3)
    mid_rows(0)
    level("W2", 0, 2)
    mid_rows(1)
    level("W2", 1, 2)
    level("W1", 0, 4)
    level("W1", 1, 4)
    spread(0)
    spread_end(0)
    ff_in_half(0)
    spread(1)
    level("W2", 0, 3)
    ff_group(0, 0)
    ff_group(1, 0)
    ff_chip(0, 0)
    level("W2", 1, 3)
    spread_end(1)
    ff_in_half(1)
    ff_chip(1, 0)
    ff_group(0, 1)
    level("W2", 0, 4)
    ff_group(1, 1)
    ff_chip(0, 1)
    level("W2", 1, 4)
    ff_group(2, 0)
    ff_chip(1, 1)
    ff_group(2, 1)
    ff_chip(2, 0)
    ff_end(0, 0)
    ff_chip(2, 1)
    ff_end(1, 0)
    ff_end(0, 1)
    ff_end(1, 1)
    ff_end(2, 0)
    ff_end(2, 1)

    tree_rows = 2 * (BLOCKS - 1) * THIRD + len(LINKS) * THIRD
    over_rows = 2 * len(PASSED) * THIRD
    shared_rows = sum((3 if k < NEAR else 2) * THIRD for k in SHARED)
    sent(cat.at[pl.ds(0, tree_rows + over_rows + shared_rows), :], ls.at[0])
    sent(w1.at[pl.ds(0, BLOCKS - 1)], s1.at[0])
    sent(w2.at[pl.ds(0, BLOCKS - 1)], s2.at[0])
    sent(sib, ps.at[0])
    sent(xs, ps.at[1])
    sent(fin.at[pl.ds(0, 2 * SIDE - 1)], ps.at[2])
    sent(psib, ps.at[3])
    sent(pxs, ps.at[4])


def body(
    stream,
    query_nope,
    query_rope,
    latent,
    rope_key,
    latent_gain,
    key_up,
    value_up,
    out_gain,
    out_weight,
    norm_gain,
    ff_in,
    ff_out,
):
    near, far = rotary_tables()
    vmem = pl.BlockSpec(memory_space=pltpu.VMEM)
    hbm = pl.BlockSpec(memory_space=pl.ANY)
    dma = pltpu.SemaphoreType.DMA
    return pl.pallas_call(
        kernel,
        out_shape=jax.ShapeDtypeStruct((OWN, D), BF16),
        in_specs=[hbm, hbm, hbm, hbm, hbm, vmem, hbm, hbm, vmem, hbm, vmem, hbm, hbm, hbm, hbm],
        out_specs=vmem,
        scratch_shapes=[
            pltpu.VMEM((2 * ROWS, NOPE), BF16),
            pltpu.VMEM((2, ROPE, ROWS), BF16),
            pltpu.VMEM((ROWS, LATENT), BF16),
            pltpu.VMEM((ROPE, ROWS), BF16),
            pltpu.VMEM((2 * LATENT, NOPE), BF16),
            pltpu.VMEM((2 * LATENT, VDIM), BF16),
            pltpu.VMEM((ROPE, ROWS), F32),
            pltpu.VMEM((BLOCKS * PAIR, PACK), BF16),
            pltpu.VMEM((BLOCKS, D // BLOCKS, HID), BF16),
            pltpu.VMEM((BLOCKS, HID, D // BLOCKS), BF16),
            pltpu.VMEM((2 * ROWS, LATENT + 128), BF16),
            pltpu.VMEM((2 * ROWS, LATENT + 128), BF16),
            pltpu.VMEM((2 * ROWS, UNIT), F32),
            pltpu.VMEM((2 * ROWS, UNIT), F32),
            pltpu.VMEM((2 * ROWS, UNIT), BF16),
            pltpu.VMEM((2 * ROWS, UNIT), BF16),
            pltpu.VMEM((2 * ROWS, LATENT), F32),
            pltpu.VMEM((2 * ROWS, 128), F32),
            pltpu.VMEM((2 * ROWS, 128), F32),
            pltpu.VMEM((ROPE, 128), F32),
            pltpu.VMEM((OWN, D), BF16),
            pltpu.VMEM((2 * VDIM, D), BF16),
            pltpu.VMEM((SIDE, 2, OWN, EXT), BF16),
            pltpu.VMEM((SIDE, OWN, EXT), BF16),
            pltpu.VMEM((SIDE - 1, OWN, EXT), BF16),
            pltpu.VMEM((SIDE - 1, OWN, EXT), BF16),
            pltpu.VMEM((2 * SIDE, OWN, D), BF16),
            pltpu.VMEM((ROWS, HID), BF16),
            pltpu.VMEM((SIDE, 2, OWN, D), BF16),
            pltpu.VMEM((SIDE, OWN, D), BF16),
            pltpu.VMEM((SIDE - 1, OWN, D), BF16),
            pltpu.VMEM((SIDE - 1, OWN, D), BF16),
            pltpu.VMEM((OWN, D), F32),
            pltpu.VMEM((OWN, D), F32),
            pltpu.VMEM((OWN, 128), F32),
            pltpu.VMEM((2 * ROWS, NOPE), F32),
            pltpu.VMEM((2 * LATENT, NOPE), F32),
            dma((1,)),
            dma((3,)),
            dma((3,)),
            dma((12,)),
            dma((1,)),
            dma((NMSG,)),
            dma((1,)),
            dma((8,)),
            dma((1,)),
            dma((8,)),
            dma((4,)),
            dma((5,)),
            dma((2, 2)),
            dma((2, 4)),
            dma((GROUPS, 2, 2)),
        ],
        compiler_params=pltpu.CompilerParams(
            collective_id=0, has_side_effects=True, vmem_limit_bytes=60 * 1024 * 1024
        ),
    )(
        stream,
        query_nope.reshape(2 * ROWS, NOPE),
        jnp.transpose(query_rope, (1, 2, 0)),
        latent,
        jnp.transpose(rope_key, (1, 0)),
        latent_gain.reshape(1, LATENT),
        key_up.reshape(2 * LATENT, NOPE),
        value_up.reshape(2 * LATENT, VDIM),
        out_gain.reshape(1, 2 * VDIM),
        out_weight,
        norm_gain.reshape(1, D),
        ff_in,
        ff_out,
        jnp.asarray(near),
        jnp.asarray(far),
    )


def solution(mesh):
    placed = (
        P(("sp", "tp"), None),
        P("sp", "tp", None),
        P("sp", "tp", None),
        P("sp", None),
        P("sp", None),
        P(),
        P(None, "tp", None),
        P(None, "tp", None),
        P("tp"),
        P("tp", None),
        P(),
        P("sp", "tp"),
        P("tp", "sp"),
    )
    return jax.shard_map(
        body, mesh=mesh, in_specs=placed, out_specs=P(("sp", "tp"), None), check_vma=False
    )
```

time: 89.6 us -> 81.5 us (0.910)
  Pallas kernels: 87.8 us -> 79.7 us
    pallas_call x1, Pallas kernels: 87.8 us -> 79.7 us  [body(): pl.pallas_call(kernel, out_shape=jax.ShapeDtypeStruct((OWN, D), BF16), in...]
where the time goes in v3:
time: 81.5 us; the launch traced here: 81.3 us
  Pallas kernels  79.7 us (98%)
  local copies, waits for them, and re-layouts  1.62 us (2%)
    pallas_call x1, Pallas kernels, body(): pl.pallas_call(kernel, out_shape=jax.ShapeDtypeStruct((OWN, D), BF16), in...  79.7 us

profile of v3, /device:TPU:1, one launch (start us, length us, event | category | flops | bytes accessed | tf_op | source)
XLA Modules:
  0.0 81.3 jit_solution(8222455318454973625)
XLA Ops:
  0.0 79.7 %shard_map.145 = bf16[48,2048]{1,0:T(8,128)(2,1)} custom-call(bf16[48,2048]{1,0:T(8,128)(2,1)} %stream_in.1, bf16[768,128]{1,0:T(8,128)(2,1)} %bitcast.10, bf16[2,64,384]{2,1,0:T(8,128)(2,1)} %bitcast.11, bf16[384,512]{1,0:T(8,128)(2,1)} %latent_in.1, bf16[64,384]{1,0:T(8,128)(2,1)} %bitcast.12, f32[1,512]{1,0:T(1,128)} %bitcast.14, ...), custom_call_target="tpu_custom_call" | custom-call | tf_op jit(solution)/shard_map/pallas_call | solution.py:698
  79.7 1.6 %copy.17 = bf16[48,2048]{1,0:T(8,128)(2,1)} copy(bf16[48,2048]{1,0:T(8,128)(2,1)} %shard_map.145) | data formatting | bytes 393216

commit v4 on v3

--- a/solution.py
+++ b/solution.py
@@ -93,8 +93,8 @@
         _row += _rows
 assert _row == BLOCKS * PAIR
 
-PARTS = ((0, 32), (32, 48))
-EDGES = (0, 5, 11, 16)
+PARTS = ((0, 16), (16, 32), (32, 48))
+EDGES = (0, 5, 11, 15, 16)
 GROUPS = len(EDGES) - 1
 
 
@@ -116,17 +116,20 @@
     qr_in,
     latent_in,
     kr_in,
-    lat_gain,
+    lat_gain_in,
     key_up_in,
     value_up_in,
-    out_gain,
+    out_gain_in,
     out_w_in,
-    norm_gain,
+    norm_gain_in,
     ff_in,
     ff_out,
     near_in,
     far_in,
     out,
+    lat_gain,
+    out_gain,
+    norm_gain,
     qn,
     qr_t,
     latent,
@@ -216,7 +219,10 @@
         local(far_in.at[sp], far, 0),
         local(near_in, near, 6),
         local(kr_in, kr_t, 7),
+        local(lat_gain_in, lat_gain, 12),
     ]
+    og_copy = local(out_gain_in, out_gain, 13)
+    ng_copy = local(norm_gain_in, norm_gain, 14)
     early2 = [local(qn_in, qn, 8), local(key_up_in, key_up, 9), local(qr_in, qr_t, 10)]
     vu_copy = local(value_up_in, value_up, 11)
     w1_copy = local(ff_in, w1.at[sp], 1)
@@ -429,40 +435,44 @@
             c = slice(k * 128, (k + 1) * 128)
             acc[:, c] = acc[:, c] * fade + mixed[:, c]
 
-    def attend(row, count, between=()):
+    def attend(row, count, between=None):
         sa[:, 0:count] = score(qa, row, count, 0)
         sb[:, 0:count] = score(qb, row, count, LATENT)
         weigh(sa, pa, row, count, 0)
-        for g, half, k in between:
-            level(g, half, k)
+        if between is not None:
+            between()
         weigh(sb, pb, row, count, LATENT + 128)
+
+    def last_latents():
+        level("L", 0, 4)
+        level("L", 1, 4)
+        level("W1", 1, 1)
 
     level("L", 0, 1)
     level("L", 1, 1)
-    begin("W1", 0)
     rest()
     need([0], [])
-    attend(0, 768)
+    attend(0, 768, lambda: begin("W1", 0))
     level("L", 0, 2)
     level("L", 1, 2)
-    begin("W1", 1)
     need([1], [])
-    attend(768, 768)
+    attend(768, 768, lambda: begin("W1", 1))
     level("L", 0, 3)
     level("L", 1, 3)
     level("W1", 0, 1)
     begin("W2", 0)
     pass_over(0)
     need([2], [0])
-    attend(1536, 1024, [("L", 0, 4), ("L", 1, 4), ("W1", 1, 1)])
+    attend(1536, 1024, last_latents)
     begin("W2", 1)
     pass_over(1)
     pass_over(2)
     need([3], [1, 2])
-    attend(2560, 512, [("W1", 0, 2)])
+    attend(2560, 512, lambda: level("W1", 0, 2))
 
     out_lat = (acc[...] / jnp.sum(l_run[...], axis=1, keepdims=True)).astype(BF16)
     vu_copy.wait()
+    og_copy.wait()
     wide2[...] = value_up[...].astype(F32)
     squares = jnp.zeros((ROWS, 1), F32)
     gated = []
@@ -616,52 +626,76 @@
     def sent(v, sem):
         remote(v, v, sem, sem, sibling).wait_send()
 
-    swap(0).start()
-    swap(1).start()
+    for p in range(len(PARTS)):
+        swap(p).start()
     level("W1", 1, 2)
-    level("W2", 0, 1)
     chip_send(0)
     chip_send(1)
-    level("W2", 1, 1)
+    chip_send(2)
+    level("W2", 0, 1)
     st_copy.wait()
     w1_copy.wait()
     w2_copy.wait()
+    ng_copy.wait()
     level("W1", 0, 3)
+    level("W2", 1, 1)
+    mid_rows(0)
     level("W1", 1, 3)
-    mid_rows(0)
+    mid_rows(1)
+    mid_rows(2)
     level("W2", 0, 2)
-    mid_rows(1)
+    spread(0)
     level("W2", 1, 2)
     level("W1", 0, 4)
     level("W1", 1, 4)
-    spread(0)
     spread_end(0)
     ff_in_half(0)
+    ff_group(0, 0)
     spread(1)
-    level("W2", 0, 3)
-    ff_group(0, 0)
     ff_group(1, 0)
     ff_chip(0, 0)
-    level("W2", 1, 3)
     spread_end(1)
     ff_in_half(1)
     ff_chip(1, 0)
     ff_group(0, 1)
-    level("W2", 0, 4)
+    level("W2", 0, 3)
+    spread(2)
     ff_group(1, 1)
     ff_chip(0, 1)
-    level("W2", 1, 4)
+    spread_end(2)
+    ff_in_half(2)
+    ff_chip(1, 1)
+    ff_group(0, 2)
+    level("W2", 1, 3)
+    ff_group(1, 2)
+    ff_chip(0, 2)
+    level("W2", 0, 4)
     ff_group(2, 0)
-    ff_chip(1, 1)
+    ff_chip(1, 2)
     ff_group(2, 1)
     ff_chip(2, 0)
+    ff_group(2, 2)
+    ff_chip(2, 1)
+    level("W2", 1, 4)
+    ff_group(3, 0)
+    ff_chip(2, 2)
+    ff_group(3, 1)
+    ff_group(3, 2)
     ff_end(0, 0)
-    ff_chip(2, 1)
+    ff_end(0, 1)
+    ff_chip(3, 0)
+    ff_chip(3, 1)
+    ff_chip(3, 2)
     ff_end(1, 0)
-    ff_end(0, 1)
     ff_end(1, 1)
+    ff_end(0, 2)
+    ff_end(1, 2)
     ff_end(2, 0)
     ff_end(2, 1)
+    ff_end(2, 2)
+    ff_end(3, 0)
+    ff_end(3, 1)
+    ff_end(3, 2)
 
     tree_rows = 2 * (BLOCKS - 1) * THIRD + len(LINKS) * THIRD
     over_rows = 2 * len(PASSED) * THIRD
@@ -698,9 +732,12 @@
     return pl.pallas_call(
         kernel,
         out_shape=jax.ShapeDtypeStruct((OWN, D), BF16),
-        in_specs=[hbm, hbm, hbm, hbm, hbm, vmem, hbm, hbm, vmem, hbm, vmem, hbm, hbm, hbm, hbm],
+        in_specs=[hbm] * 15,
         out_specs=vmem,
         scratch_shapes=[
+            pltpu.VMEM((1, LATENT), F32),
+            pltpu.VMEM((1, 2 * VDIM), F32),
+            pltpu.VMEM((1, D), F32),
             pltpu.VMEM((2 * ROWS, NOPE), BF16),
             pltpu.VMEM((2, ROPE, ROWS), BF16),
             pltpu.VMEM((ROWS, LATENT), BF16),
@@ -741,7 +778,7 @@
             dma((1,)),
             dma((3,)),
             dma((3,)),
-            dma((12,)),
+            dma((15,)),
             dma((1,)),
             dma((NMSG,)),
             dma((1,)),
@@ -750,9 +787,9 @@
             dma((8,)),
             dma((4,)),
             dma((5,)),
-            dma((2, 2)),
-            dma((2, 4)),
-            dma((GROUPS, 2, 2)),
+            dma((3, 2)),
+            dma((3, 4)),
+            dma((GROUPS, 3, 2)),
         ],
         compiler_params=pltpu.CompilerParams(
             collective_id=0, has_side_effects=True, vmem_limit_bytes=60 * 1024 * 1024

time: 81.5 us -> 79.2 us (0.972)
  Pallas kernels: 79.7 us -> 77.4 us
    pallas_call x1, Pallas kernels: 79.7 us -> 77.4 us  [body(): pl.pallas_call(kernel, out_shape=jax.ShapeDtypeStruct((OWN, D), BF16), in...]
where the time goes in v4:
time: 79.2 us; the launch traced here: 79.1 us
  Pallas kernels  77.4 us (98%)
  local copies, waits for them, and re-layouts  1.62 us (2%)
    pallas_call x1, Pallas kernels, body(): pl.pallas_call(kernel, out_shape=jax.ShapeDtypeStruct((OWN, D), BF16), in...  77.4 us
    unnamed x1, local copies, waits for them, and re-layouts  1.62 us

profile of v4, /device:TPU:1, one launch (start us, length us, event | category | flops | bytes accessed | tf_op | source)
XLA Modules:
  0.0 79.1 jit_solution(11886213910335839631)
XLA Ops:
  0.0 77.4 %shard_map.145 = bf16[48,2048]{1,0:T(8,128)(2,1)} custom-call(bf16[48,2048]{1,0:T(8,128)(2,1)} %stream_in.1, bf16[768,128]{1,0:T(8,128)(2,1)} %bitcast.10, bf16[2,64,384]{2,1,0:T(8,128)(2,1)} %bitcast.11, bf16[384,512]{1,0:T(8,128)(2,1)} %latent_in.1, bf16[64,384]{1,0:T(8,128)(2,1)} %bitcast.12, f32[1,512]{1,0:T(1,128)} %bitcast.14, ...), custom_call_target="tpu_custom_call" | custom-call | tf_op jit(solution)/shard_map/pallas_call | solution.py:732
  77.4 1.6 %copy.17 = bf16[48,2048]{1,0:T(8,128)(2,1)} copy(bf16[48,2048]{1,0:T(8,128)(2,1)} %shard_map.145) | data formatting | bytes 393216

commit v5 on v4

--- a/solution.py
+++ b/solution.py
@@ -93,7 +93,8 @@
         _row += _rows
 assert _row == BLOCKS * PAIR
 
-PARTS = ((0, 16), (16, 32), (32, 48))
+PARTS = ((0, 16), (16, 32), (32, 48), (0, 48))
+ALL = len(PARTS) - 1
 EDGES = (0, 5, 11, 15, 16)
 GROUPS = len(EDGES) - 1
 
@@ -588,15 +589,21 @@
         )
 
     def ff_group(g, p):
-        first, last = PARTS[p]
-        for n in range(EDGES[g], EDGES[g + 1]):
-            f = ORDER[n]
+        n = EDGES[g]
+        while n < EDGES[g + 1]:
+            many = min(2, EDGES[g + 1] - n)
+            weights = jnp.concatenate([w2[block_at(*ORDER[k])] for k in range(n, n + many)], axis=1)
+            first, last = PARTS[p]
             piece = jnp.dot(
-                act[8 * first : 8 * last, :], w2[block_at(*f)], preferred_element_type=F32
+                act[8 * first : 8 * last, :], weights, preferred_element_type=F32
             ).astype(BF16)
-            part[:, :, first:last, n * 128 : (n + 1) * 128] = piece.reshape(
-                SIDE, 2, last - first, 128
-            )
+            for q in range(ALL) if p == ALL else (p,):
+                start, stop = PARTS[q]
+                rows = piece[8 * (start - first) : 8 * (stop - first)]
+                part[:, :, start:stop, n * 128 : (n + many) * 128] = rows.reshape(
+                    SIDE, 2, stop - start, many * 128
+                )
+            n += many
         swap_part(g, p).start()
 
     def ff_chip(g, p):
@@ -626,12 +633,12 @@
     def sent(v, sem):
         remote(v, v, sem, sem, sibling).wait_send()
 
-    for p in range(len(PARTS)):
+    for p in range(ALL):
         swap(p).start()
-    level("W1", 1, 2)
     chip_send(0)
     chip_send(1)
     chip_send(2)
+    level("W1", 1, 2)
     level("W2", 0, 1)
     st_copy.wait()
     w1_copy.wait()
@@ -669,33 +676,21 @@
     level("W2", 1, 3)
     ff_group(1, 2)
     ff_chip(0, 2)
+    ff_group(2, ALL)
     level("W2", 0, 4)
-    ff_group(2, 0)
     ff_chip(1, 2)
-    ff_group(2, 1)
-    ff_chip(2, 0)
-    ff_group(2, 2)
-    ff_chip(2, 1)
+    ff_chip(2, ALL)
     level("W2", 1, 4)
-    ff_group(3, 0)
-    ff_chip(2, 2)
-    ff_group(3, 1)
-    ff_group(3, 2)
+    ff_group(3, ALL)
     ff_end(0, 0)
+    ff_end(1, 0)
     ff_end(0, 1)
-    ff_chip(3, 0)
-    ff_chip(3, 1)
-    ff_chip(3, 2)
-    ff_end(1, 0)
     ff_end(1, 1)
+    ff_chip(3, ALL)
     ff_end(0, 2)
     ff_end(1, 2)
-    ff_end(2, 0)
-    ff_end(2, 1)
-    ff_end(2, 2)
-    ff_end(3, 0)
-    ff_end(3, 1)
-    ff_end(3, 2)
+    ff_end(2, ALL)
+    ff_end(3, ALL)
 
     tree_rows = 2 * (BLOCKS - 1) * THIRD + len(LINKS) * THIRD
     over_rows = 2 * len(PASSED) * THIRD
@@ -789,7 +784,7 @@
             dma((5,)),
             dma((3, 2)),
             dma((3, 4)),
-            dma((GROUPS, 3, 2)),
+            dma((GROUPS, 4, 2)),
         ],
         compiler_params=pltpu.CompilerParams(
             collective_id=0, has_side_effects=True, vmem_limit_bytes=60 * 1024 * 1024

time: 79.2 us -> 79.1 us (level)
  no operation moved by 1% of the time
where the time goes in v5:
time: 79.1 us; the launch traced here: 78.9 us
  Pallas kernels  77.3 us (98%)
  local copies, waits for them, and re-layouts  1.62 us (2%)
    pallas_call x1, Pallas kernels, body(): pl.pallas_call(kernel, out_shape=jax.ShapeDtypeStruct((OWN, D), BF16), in...  77.3 us
    unnamed x1, local copies, waits for them, and re-layouts  1.62 us

profile of v5, /device:TPU:1, one launch (start us, length us, event | category | flops | bytes accessed | tf_op | source)
XLA Modules:
  0.0 78.9 jit_solution(1589707977636730545)
XLA Ops:
  0.0 77.3 %shard_map.145 = bf16[48,2048]{1,0:T(8,128)(2,1)} custom-call(bf16[48,2048]{1,0:T(8,128)(2,1)} %stream_in.1, bf16[768,128]{1,0:T(8,128)(2,1)} %bitcast.10, bf16[2,64,384]{2,1,0:T(8,128)(2,1)} %bitcast.11, bf16[384,512]{1,0:T(8,128)(2,1)} %latent_in.1, bf16[64,384]{1,0:T(8,128)(2,1)} %bitcast.12, f32[1,512]{1,0:T(1,128)} %bitcast.14, ...), custom_call_target="tpu_custom_call" | custom-call | tf_op jit(solution)/shard_map/pallas_call | solution.py:727
  77.3 1.6 %copy.17 = bf16[48,2048]{1,0:T(8,128)(2,1)} copy(bf16[48,2048]{1,0:T(8,128)(2,1)} %shard_map.145) | data formatting | bytes 393216
